TPU v7x, 256 devices: a whole 4x4x8 slice. The times are simulated.
256 devices in a mesh: ep: 128 (over z, y, x), tp: 2 (over core).
Axes of the slice: x: 4, y: 4, z: 8, core: 2. Of those that a mesh axis runs over, the one named last changes fastest.
Arguments:
- tokens: bfloat16 [2048, 2048], P('ep'), may hold values from -6 to 6
- cache_keys: bfloat16 [2048, 2, 64, 1024], P('ep', 'tp'), may hold values from -6 to 6
- cache_values: bfloat16 [2048, 2, 64, 1024], P('ep', 'tp'), may hold values from -6 to 6
- cache_lengths: int32 [2048], P('ep'), may hold values from 1 to 1024, as said below
- norm_in: float32 [2048], replicated, may hold values from 0.1 to 1.9
- w_query: bfloat16 [2048, 512], P(None, 'tp'), may hold values from -0.125 to 0.125
- w_key: bfloat16 [2048, 128], P(None, 'tp'), may hold values from -0.125 to 0.125
- w_value: bfloat16 [2048, 128], P(None, 'tp'), may hold values from -0.125 to 0.125
- stick_bias: float32 [8], P('tp'), may hold values from -8 to -1.5
- w_output: bfloat16 [512, 2048], P('tp'), may hold values from -0.75 to 0.75
- norm_mid: float32 [2048], replicated, may hold values from 0.1 to 1.9
- routes: int32 [2048, 6], P('ep'), may hold values from 0 to 127, all different within a row; in each aligned block of 16 rows (0 to 15, 16 to 31, ...) at most 2 rows name the same one
- route_weights: float32 [2048, 6], P('ep'), may hold values from 0.1 to 1
- expert_gate: bfloat16 [128, 2048, 512], P('ep', None, 'tp'), may hold values from -0.125 to 0.125
- expert_up: bfloat16 [128, 2048, 512], P('ep', None, 'tp'), may hold values from -0.125 to 0.125
- expert_down: bfloat16 [128, 512, 2048], P('ep', 'tp'), may hold values from -0.25 to 0.25
- dense_gate: bfloat16 [2048, 256], P('ep'), may hold values from -0.125 to 0.125
- dense_up: bfloat16 [2048, 256], P('ep'), may hold values from -0.125 to 0.125
- dense_down: bfloat16 [256, 2048], P(None, 'ep'), may hold values from -0.375 to 0.375
- mix_gate: float32 [2048], replicated, may hold values from -0.125 to 0.125
- norm_out: float32 [2048], replicated, may hold values from 0.1 to 1.9
Outputs:
- mixed: bfloat16 [2048, 2048], P('ep')
- fresh_keys: bfloat16 [2048, 128], P('ep', 'tp')
- fresh_values: bfloat16 [2048, 128], P('ep', 'tp')
Inputs may be any that keep to these rules, and one draw needn't show every extreme that they name: `cache_lengths`: positions at or past a sequence's length are not read. Among the sequences of one index of ep some sequence has length 1024. `routes`: each row names 6 different experts; among the rows of one index of ep (aligned blocks of 16 rows) no expert is named by more than 2 rows, and that bound is reached.
All inputs are finite; a program needn't handle non-finite values.
Results may differ from a plain program's by a relative error of at most 0.015.
Values may be sent and summed in bfloat16 or wider, within the bound.
A program may use at most 64 MiB of HBM per device.

v0:
```python
import jax
import jax.numpy as jnp
from jax import lax
from jax.sharding import Mesh
from jax.sharding import PartitionSpec as P

EP = ("ep_0", "ep_1", "ep_2")


def sent_to_all(value, axis):
    copies = jnp.broadcast_to(value, (lax.axis_size(axis), *value.shape))
    return lax.all_to_all(copies, axis, split_axis=0, concat_axis=0, tiled=True)


def taken_together(value, axis):
    everything = sent_to_all(value, axis)
    return jnp.sum(everything, axis=0)


def in_order(tiles, dim):
    tiles = jnp.moveaxis(tiles, 0, dim)
    lengths = tiles.shape
    return tiles.reshape(*lengths[:dim], lengths[dim] * lengths[dim + 1], *lengths[dim + 2 :])


def gather_directly(value, axis, dim):
    tiles = sent_to_all(value, axis)
    return in_order(tiles, dim)


def split_up(value, dim, size):
    lengths = value.shape
    tiles = value.reshape(*lengths[:dim], size, lengths[dim] // size, *lengths[dim + 1 :])
    return jnp.moveaxis(tiles, dim, 0)


def sent_and_summed(value, axis, dim):
    size = lax.axis_size(axis)
    tiles = lax.all_to_all(split_up(value, dim, size), axis, 0, 0, tiled=True)
    return jnp.sum(tiles.astype(jnp.float32), axis=0)


def moved_by_axis(tiles, axes, order):
    lengths = [lax.axis_size(a) for a in axes]
    tiles = tiles.reshape(*lengths, *tiles.shape[1:])
    for k in order:
        tiles = lax.all_to_all(tiles, axes[k], split_axis=k, concat_axis=k, tiled=True)
    return tiles.reshape(-1, *tiles.shape[len(axes) :])


def exchange_by_axis(value, axes, order, split_dim, concat_dim):
    tiles = split_up(value, split_dim, lax.axis_size(axes))
    return in_order(moved_by_axis(tiles, axes, order), concat_dim)


def sent_together(arrays, axis, dim, along):
    ends, at = ([], 0)
    for a in arrays[:-1]:
        at += a.shape[along]
        ends.append(at)
    both = jnp.concatenate(arrays, axis=along)
    return tuple(jnp.split(lax.all_gather(both, axis, axis=dim, tiled=True), ends, axis=along))


def gathered_by_axis(value, axes, dim):
    out = value
    for number in range(len(axes) - 1, -1, -1):
        out = lax.all_gather(out, axes[number], axis=dim, tiled=True)
    return out


def layer_norm(values, gain):
    floats = values.astype(jnp.float32)
    center = jnp.mean(floats, -1, keepdims=True)
    spread = jnp.mean(jnp.square(floats - center), -1, keepdims=True)
    return (floats - center) * lax.rsqrt(spread + 1e-05) * gain


def later_positions(log_keep):
    length = log_keep.shape[-1]
    span = 128
    count = length // span
    lead = log_keep.shape[:-1]
    blocks = log_keep.reshape(lead + (count, span))
    inner = jnp.arange(span)
    within_table = (inner[:, None] > inner[None, :]).astype(jnp.float32)
    within = jnp.einsum("...nb,bc->...nc", blocks, within_table, precision=lax.Precision.HIGHEST)
    totals = jnp.sum(blocks, axis=-1)
    outer = jnp.arange(count)
    outer_table = (outer[:, None] > outer[None, :]).astype(jnp.float32)
    carried = jnp.einsum("...m,mn->...n", totals, outer_table, precision=lax.Precision.HIGHEST)
    return (within + carried[..., None]).reshape(lead + (length,))


def shards(
    tokens,
    cache_keys,
    cache_values,
    cache_lengths,
    norm_in,
    w_query,
    w_key,
    w_value,
    stick_bias,
    w_output,
    norm_mid,
    routes,
    route_weights,
    expert_gate,
    expert_up,
    expert_down,
    dense_gate,
    dense_up,
    dense_down,
    mix_gate,
    norm_out,
):
    normed = layer_norm(tokens, norm_in).astype(jnp.bfloat16)
    queries = jnp.dot(normed, w_query, preferred_element_type=jnp.float32).astype(jnp.bfloat16)
    fresh_keys = jnp.dot(normed, w_key, preferred_element_type=jnp.float32).astype(jnp.bfloat16)
    fresh_values = jnp.dot(normed, w_value, preferred_element_type=jnp.float32).astype(jnp.bfloat16)
    sequences = tokens.shape[0]
    kv_local = cache_keys.shape[1]
    head_dim = cache_keys.shape[2]
    length = cache_keys.shape[3]
    heads_local = stick_bias.shape[0]
    groups = heads_local // kv_local
    query_grid = queries.reshape(sequences, kv_local, groups, head_dim)
    scores = jnp.einsum(
        "skgd,skdc->skgc", query_grid, cache_keys, preferred_element_type=jnp.float32
    ) * head_dim ** (-0.5)
    scores = scores + stick_bias.reshape(kv_local, groups)[None, :, :, None]
    visible = (jnp.arange(length)[None, :] < cache_lengths[:, None])[:, None, None, :]
    log_keep = jnp.where(visible, jax.nn.log_sigmoid(-scores), 0.0)
    later_sum = later_positions(log_keep)
    stick = jnp.where(visible, jnp.exp(jax.nn.log_sigmoid(scores) + later_sum), 0.0).astype(
        jnp.bfloat16
    )
    attended = jnp.einsum(
        "skgc,skdc->skgd", stick, cache_values, preferred_element_type=jnp.float32
    )
    attended = attended.reshape(sequences, heads_local * head_dim).astype(jnp.bfloat16)
    partial_proj = jnp.dot(attended, w_output, preferred_element_type=jnp.float32)
    projected = taken_together(partial_proj, "tp")
    hidden = layer_norm(normed.astype(jnp.float32) + projected, norm_mid).astype(jnp.bfloat16)
    width = hidden.shape[1]
    topk = routes.shape[1]
    ep_count = lax.axis_size(EP)
    experts = ep_count * expert_gate.shape[0]
    capacity = max(2, (sequences * topk + ep_count - 1) // ep_count)
    flat_routes = routes.reshape(-1)
    onehot = (flat_routes[:, None] == jnp.arange(experts)[None, :]).astype(jnp.float32)
    flat_count = flat_routes.shape[0]
    row_index = jnp.arange(flat_count)
    earlier_table = (row_index[:, None] > row_index[None, :]).astype(jnp.float32)
    before = jnp.dot(earlier_table, onehot, precision=lax.Precision.HIGHEST)
    slot_index = jnp.sum(before * onehot, axis=1).astype(jnp.int32)
    target = flat_routes * capacity + slot_index
    placement = jnp.arange(experts * capacity)[:, None] == target[None, :]
    dispatch = jnp.any(placement.reshape(experts * capacity, sequences, topk), axis=2).astype(
        jnp.bfloat16
    )
    outgoing = jnp.dot(dispatch, hidden, preferred_element_type=jnp.float32).astype(jnp.bfloat16)
    outgoing = outgoing.reshape(ep_count, capacity, width)
    half_width = width // lax.axis_size("tp")
    own_half = lax.dynamic_slice_in_dim(outgoing, lax.axis_index("tp") * half_width, half_width, 2)
    received_half = lax.all_to_all(own_half, EP, split_axis=0, concat_axis=0, tiled=True)
    received = gather_directly(received_half, "tp", 2)
    token_rows = received.reshape(-1, width)
    gate_pre = jnp.dot(token_rows, expert_gate[0], preferred_element_type=jnp.float32)
    up_pre = jnp.dot(token_rows, expert_up[0], preferred_element_type=jnp.float32)
    act = (jax.nn.silu(gate_pre) * up_pre).astype(jnp.bfloat16)
    partial_out = (
        jnp.dot(act, expert_down[0], preferred_element_type=jnp.float32)
        .astype(jnp.bfloat16)
        .reshape(ep_count, capacity, width)
    )
    expert_half = sent_and_summed(partial_out, "tp", 2).astype(jnp.bfloat16)
    returned_half = exchange_by_axis(expert_half, EP, (0, 1, 2), 0, 0)
    returned = gather_directly(returned_half, "tp", 2)
    selector = jnp.transpose(placement).astype(jnp.bfloat16)
    picked = jnp.dot(selector, returned.reshape(-1, width), preferred_element_type=jnp.float32)
    routed = jnp.sum(picked.reshape(sequences, topk, width) * route_weights[:, :, None], axis=1)
    pieces = sent_together((dense_gate, dense_up), EP, 0, 1)
    dense_pre = jnp.dot(hidden, pieces[0], preferred_element_type=jnp.float32)
    dense_lin = jnp.dot(hidden, pieces[1], preferred_element_type=jnp.float32)
    dense_act = (jax.nn.silu(dense_pre) * dense_lin).astype(jnp.bfloat16)
    dense_out = jnp.dot(
        dense_act, gathered_by_axis(dense_down, EP, 1), preferred_element_type=jnp.float32
    )
    mix_weight = jax.nn.sigmoid(
        jnp.dot(hidden.astype(jnp.float32), mix_gate, precision=lax.Precision.HIGHEST)
    )
    combined_rows = hidden.astype(jnp.float32) + routed + mix_weight[:, None] * dense_out
    mixed_rows = layer_norm(combined_rows, norm_out).astype(jnp.bfloat16)
    return (mixed_rows, fresh_keys, fresh_values)


def solution(mesh):
    split = Mesh(mesh.devices.reshape(8, 4, 4, mesh.shape["tp"]), ("ep_0", "ep_1", "ep_2", "tp"))
    return jax.shard_map(
        shards,
        mesh=split,
        in_specs=(
            P(EP, None),
            P(EP, "tp", None, None),
            P(EP, "tp", None, None),
            P(EP),
            P(),
            P(None, "tp"),
            P(None, "tp"),
            P(None, "tp"),
            P("tp"),
            P("tp", None),
            P(),
            P(EP, None),
            P(EP, None),
            P(EP, None, "tp"),
            P(EP, None, "tp"),
            P(EP, "tp", None),
            P(EP, None),
            P(EP, None),
            P(None, EP),
            P(),
            P(),
        ),
        out_specs=(P(EP, None), P(EP, "tp"), P(EP, "tp")),
        check_vma=False,
    )
```

profile of v0, /device:TPU:4, one launch (start us, length us, event | category | flops | bytes accessed | tf_op | source)
XLA Modules:
  0.0 178.2 jit_solution(13516944446550676727)
XLA Ops:
  7.2 1.5 pad_maximum_fusion
  8.7 1.0 convert_reduce_fusion
  9.7 1.0 fusion.46
  10.7 1.6 convolution_convert_fusion.2
  12.3 0.1 reshape.188
  12.4 0.7 iota_compare_fusion.3
  13.2 2.0 %fusion.37 = (f32[16,4,1024]{2,1,0:T(4,128)S(1)}, f32[16,4,1024]{2,1,0:T(4,128)}) fusion(pred[16,1024]{1,0:T(8,128)(4,1)S(1)} %iota_compare_fusion.3, f32[4]{0:T(128)} %param.29, bf16[16,4,64]{2,1,0:T(4,128)(2,1)S(1)} %reshape.188, bf16[16,1,64,1024]{3,2,1,0:T(8,128)(2,1)S(1)} %copy-done), kind=kOutput, calls=%fused_computation.44 | convolution fusion | flops 9043968 | bytes 2646032 | tf_op jit(solution)/shard_map/skgd,skdc->skgc/dot_general | solution.py:129
  15.1 0.1 reshape.190
  15.2 0.2 reduce_sum.104
  15.4 0.2 fusion.57
  15.6 0.1 copy.65
  15.7 1.0 convolution_add_fusion
  16.7 1.0 reshape.191
  17.7 2.4 %fusion.14 = bf16[16,4,64]{2,1,0:T(4,128)(2,1)S(1)} fusion(bf16[16,1,64,1024]{3,2,1,0:T(8,128)(2,1)} %param.23, f32[16,4,1024]{2,1,0:T(4,128)S(1)} %reshape.191, f32[16,4,1024]{2,1,0:T(4,128)} %get-tuple-element.4, pred[16,1024]{1,0:T(8,128)(4,1)S(1)} %iota_compare_fusion.3), kind=kOutput, calls=%fused_computation.17 | convolution fusion | flops 9113600 | bytes 2646016 | tf_op jit(solution)/shard_map/skgc,skdc->skgd/dot_general | solution.py:139
  20.1 0.1 convert_element_type.75
  20.2 0.2 fusion.77
  20.5 0.7 broadcast_in_dim.21
  21.2 3.4 %all-to-all-start = ((f32[2,16,2048]{2,1,0:T(8,128)}), f32[2,16,2048]{2,1,0:T(8,128)S(1)}, u32[]{:S(2)}, u32[]{:S(2)}) async-start(f32[2,16,2048]{2,1,0:T(8,128)} %broadcast_in_dim.21), calls=%async_computation | async-start | bytes 524288 | tf_op jit(solution)/shard_map/all_to_all | solution.py:12
  24.7 0.1 copy.66
  24.8 0.1 reshape.193
  24.9 0.3 fusion.13
  25.2 0.2 copy-done.10
  25.4 0.1 copy.67
  25.5 0.7 all-to-all-done
  26.3 0.2 fusion.56
  26.6 0.2 multiply_reduce_fusion.1
  26.8 0.1 multiply_convert_fusion.1
  26.9 0.5 convolution_convert_fusion
  27.4 1.5 reshape.194
  28.9 1.4 constant_dynamic-slice_fusion
  30.3 33.7 %all_to_all.40 = bf16[128,2,1024]{2,1,0:T(2,128)(2,1)S(1)} all-to-all(bf16[128,2,1024]{2,1,0:T(2,128)(2,1)S(1)} %constant_dynamic-slice_fusion), channel_id=1, replica_groups=mesh['ep_0'=8,'ep_1'=4,'ep_2'=4,'tp'=2] {'ep_0','ep_1','ep_2'}, dimensions={0} | all-to-all | bytes 1048576 | tf_op jit(solution)/shard_map/all_to_all | solution.py:167
  64.0 0.5 broadcast_in_dim.22
  64.6 4.6 %all_to_all.41 = bf16[2,128,2,1024]{3,2,1,0:T(2,128)(2,1)S(1)} all-to-all(bf16[2,128,2,1024]{3,2,1,0:T(2,128)(2,1)S(1)} %broadcast_in_dim.22), channel_id=1, replica_groups=mesh['ep_0'=8,'ep_1'=4,'ep_2'=4,'tp'=2] {'tp'}, dimensions={0} | all-to-all | bytes 2097152 | tf_op jit(solution)/shard_map/all_to_all | solution.py:12
  69.2 1.6 copy.68
  70.8 0.3 copy.76
  71.1 0.5 fusion.29
  71.5 3.8 %convolution_convert_fusion.1 = bf16[256,2048]{1,0:T(8,128)(2,1)} fusion(bf16[256,2048]{1,0:T(8,128)(2,1)S(1)} %bitcast.73, bf16[1,256,2048]{2,1,0:T(8,128)(2,1)} %param.36, bf16[1,2048,256]{2,1,0:T(8,128)(2,1)} %param.35, f32[256,256]{1,0:T(8,128)S(1)} %fusion.29), kind=kOutput, calls=%fused_computation.1 | convolution fusion | flops 537788416 | bytes 4456448 | tf_op jit(solution)/shard_map/dot_general | solution.py:174
  75.3 1.8 %reshape_reshape.16 = bf16[128,2,2,1024]{3,2,1,0:T(2,128)(2,1)S(1)} reshape(bf16[256,2048]{1,0:T(8,128)(2,1)} %convolution_convert_fusion.1) | data formatting | bytes 2097152 | tf_op jit(solution)/shard_map/reshape;reshape | solution.py:33
  77.2 0.8 copy.82
  78.0 4.7 %all_to_all.42 = bf16[2,128,2,1024]{3,2,1,0:T(2,128)(2,1)S(1)} all-to-all(bf16[2,128,2,1024]{3,2,1,0:T(2,128)(2,1)S(1)} %bitcast.76), channel_id=1, replica_groups=mesh['ep_0'=8,'ep_1'=4,'ep_2'=4,'tp'=2] {'tp'}, dimensions={0} | all-to-all | bytes 2097152 | tf_op jit(solution)/shard_map/all_to_all | solution.py:39
  82.7 3.1 %reduce_sum.109 = bf16[128,2,1024]{2,1,0:T(2,128)(2,1)} reduce(bf16[2,128,2,1024]{3,2,1,0:T(2,128)(2,1)S(1)} %all_to_all.42, bf16[]{:T(256)} %constant.40.clone.1), dimensions={0}, to_apply=%region_8.9 | reduce | flops 262144 | bytes 1572866 | tf_op jit(solution)/shard_map/reduce_sum | solution.py:40
  85.8 3.6 %all-to-all-start.4 = ((bf16[8,4,4,1,2,1024]{5,4,2,1,3,0:T(2,128)(2,1)}), bf16[8,4,4,1,2,1024]{5,4,2,1,3,0:T(2,128)(2,1)S(1)}, u32[]{:S(2)}, u32[]{:S(2)}) async-start(bf16[8,4,4,1,2,1024]{5,4,2,1,3,0:T(2,128)(2,1)} %bitcast.79), calls=%async_computation.4 | async-start | bytes 1048576 | tf_op jit(solution)/shard_map/all_to_all | solution.py:47
  89.5 13.2 %all_gather.13 = bf16[256,64]{0,1:T(8,128)(2,1)S(1)} all-gather(bf16[256,16]{0,1:T(8,128)(2,1)S(1)} %copy-done.7), channel_id=1, replica_groups=mesh['ep_0'=8,'ep_1'=4,'ep_2'=4,'tp'=2] {'ep_2'}, dimensions={1}, use_global_device_ids=true | all-gather | bytes 40960 | tf_op jit(solution)/shard_map/all_gather | solution.py:68
  102.7 12.8 %all_gather.14 = bf16[256,256]{0,1:T(8,128)(2,1)} all-gather(bf16[256,64]{0,1:T(8,128)(2,1)S(1)} %all_gather.13), channel_id=1, replica_groups=mesh['ep_0'=8,'ep_1'=4,'ep_2'=4,'tp'=2] {'ep_1'}, dimensions={1}, use_global_device_ids=true | all-gather | bytes 163840 | tf_op jit(solution)/shard_map/all_gather | solution.py:68
  115.6 1.3 copy.70
  116.8 3.6 %all-to-all-start.5 = ((bf16[8,4,4,1,2,1024]{5,4,2,0,3,1:T(2,128)(2,1)}), bf16[8,4,4,1,2,1024]{5,4,2,0,3,1:T(2,128)(2,1)S(1)}, u32[]{:S(2)}, u32[]{:S(2)}) async-start(bf16[8,4,4,1,2,1024]{5,4,2,0,3,1:T(2,128)(2,1)} %copy.70), calls=%async_computation.5 | async-start | bytes 1048576 | tf_op jit(solution)/shard_map/all_to_all | solution.py:47
  120.6 0.8 convolution_convert_fusion.3
  121.4 7.1 %all-to-all-done.5 = bf16[8,4,4,1,2,1024]{5,4,2,0,3,1:T(2,128)(2,1)S(1)} async-done(((bf16[8,4,4,1,2,1024]{5,4,2,0,3,1:T(2,128)(2,1)}), bf16[8,4,4,1,2,1024]{5,4,2,0,3,1:T(2,128)(2,1)S(1)}, u32[]{:S(2)}, u32[]{:S(2)}) %all-to-all-start.5) | async-done | bytes 524320 | tf_op jit(solution)/shard_map/all_to_all | solution.py:47
  128.5 1.3 copy.71
  129.9 5.5 %all-to-all-start.6 = ((bf16[8,4,4,1,2,1024]{5,4,1,0,3,2:T(2,128)(2,1)}), bf16[8,4,4,1,2,1024]{5,4,1,0,3,2:T(2,128)(2,1)S(1)}, u32[]{:S(2)}, u32[]{:S(2)}) async-start(bf16[8,4,4,1,2,1024]{5,4,1,0,3,2:T(2,128)(2,1)} %copy.71), calls=%async_computation.6 | async-start | bytes 1048576 | tf_op jit(solution)/shard_map/all_to_all | solution.py:47
  135.4 0.1 fusion.21
  135.5 0.9 convolution_convert_fusion.4
  136.4 4.1 %all-to-all-done.6 = bf16[8,4,4,1,2,1024]{5,4,1,0,3,2:T(2,128)(2,1)S(1)} async-done(((bf16[8,4,4,1,2,1024]{5,4,1,0,3,2:T(2,128)(2,1)}), bf16[8,4,4,1,2,1024]{5,4,1,0,3,2:T(2,128)(2,1)S(1)}, u32[]{:S(2)}, u32[]{:S(2)}) %all-to-all-start.6) | async-done | bytes 524320 | tf_op jit(solution)/shard_map/all_to_all | solution.py:47
  140.5 0.5 copy.72
  141.0 0.5 broadcast_in_dim.23
  141.6 4.6 %all_to_all.43 = bf16[2,128,2,1024]{3,2,1,0:T(2,128)(2,1)S(1)} all-to-all(bf16[2,128,2,1024]{3,2,1,0:T(2,128)(2,1)S(1)} %broadcast_in_dim.23), channel_id=1, replica_groups=mesh['ep_0'=8,'ep_1'=4,'ep_2'=4,'tp'=2] {'tp'}, dimensions={0} | all-to-all | bytes 2097152 | tf_op jit(solution)/shard_map/all_to_all | solution.py:12
  146.2 2.6 %copy.73 = bf16[128,2,2,1024]{3,2,1,0:T(2,128)(2,1)} copy(bf16[128,2,2,1024]{3,1,0,2:T(2,128)(2,1)S(1)} %bitcast.77) | data formatting | bytes 2097152 | tf_op jit(solution)/shard_map/transpose | solution.py:21
  148.8 1.8 %reshape.197 = bf16[256,2048,1]{1,0,2:T(8,128)(2,1)S(1)} reshape(bf16[128,2,2,1024]{3,2,1,0:T(2,128)(2,1)} %copy.73) | data formatting | bytes 2097152 | tf_op jit(solution)/shard_map/reshape;reshape | solution.py:182
  150.6 0.3 fusion.5
  151.0 1.5 fusion.24
  152.4 15.5 %all-gather.5.cloned.1.call-done = bf16[256,2048]{0,1:T(8,128)(2,1)} async-done(((bf16[256,256]{0,1:T(8,128)(2,1)}), bf16[256,2048]{0,1:T(8,128)(2,1)}) %all-gather.5.cloned.1.call-update) | async-done | bytes 1048592 | tf_op jit(solution)/shard_map/all_gather | solution.py:68
  167.9 2.5 %fusion.74 = (f32[16]{0:T(128)S(1)}, f32[16,2048]{1,0:T(8,128)S(1)}) fusion(bf16[256,2048]{0,1:T(8,128)(2,1)} %all-gather.5.cloned.1.call-done, bf16[16,2048]{1,0:T(8,128)(2,1)S(1)} %multiply_convert_fusion.1, bf16[2048,512]{1,0:T(8,128)(2,1)} %all-gather.3.cloned.1.call-done, f32[16,256]{1,0:T(8,128)S(1)} %fusion.24, f32[16]{0:T(128)S(1)} %fusion.21, ...), kind=kOutput, calls=%fused_computation.99 | convolution fusion | flops 33742832 | bytes 2507328 | tf_op jit(solution)/shard_map/dot_general | solution.py:188
  170.4 0.2 multiply_reduce_fusion
  170.7 0.7 multiply_convert_fusion
  (53 shorter events, 0.6 us)
Async XLA Ops:
  7.2 6.0 %copy-start = (bf16[16,1,64,1024]{3,2,1,0:T(8,128)(2,1)S(1)}, bf16[16,1,64,1024]{3,2,1,0:T(8,128)(2,1)}, u32[]{:S(2)}) copy-start(bf16[16,1,64,1024]{3,2,1,0:T(8,128)(2,1)} %param.22) | copy-start | bytes 6291460
  7.2 143.8 %all-gather.3.cloned.1.call-start = ((), (), s32[]{:S(2)}) async-start(), calls=%async_computation.8 | async-start | bytes 2113536 | tf_op jit(solution)/shard_map/all_gather | solution.py:62
  15.7 4.5 %copy-start.2 = (bf16[256,2048]{1,0:T(8,128)(2,1)S(1)}, bf16[256,2048]{1,0:T(8,128)(2,1)}, u32[]{:S(2)}) copy-start(bf16[256,2048]{1,0:T(8,128)(2,1)} %param.30) | copy-start | bytes 3145732
  17.7 6.9 %copy-start.5 = (s32[16,6]{0,1:T(8,128)S(1)}, s32[16,6]{0,1:T(8,128)}, u32[]{:S(2)}) copy-start(s32[16,6]{0,1:T(8,128)} %param.32) | copy-start | bytes 1156
  20.1 6.2 %copy-start.1 = (bf16[16,2048]{1,0:T(8,128)(2,1)S(1)}, bf16[16,2048]{1,0:T(8,128)(2,1)}, u32[]{:S(2)}) copy-start(bf16[16,2048]{1,0:T(8,128)(2,1)} %param.21) | copy-start | bytes 196612
  20.1 6.2 %copy-start.4 = (f32[2048]{0:T(1024)S(1)}, f32[2048]{0:T(1024)}, u32[]{:S(2)}) copy-start(f32[2048]{0:T(1024)} %param.25) | copy-start | bytes 24580
  20.1 6.7 %copy-start.6 = (f32[2048]{0:T(1024)S(1)}, f32[2048]{0:T(1024)}, u32[]{:S(2)}) copy-start(f32[2048]{0:T(1024)} %param.31) | copy-start | bytes 24580
  21.2 5.0 %all-to-all-start = ((f32[2,16,2048]{2,1,0:T(8,128)}), f32[2,16,2048]{2,1,0:T(8,128)S(1)}, u32[]{:S(2)}, u32[]{:S(2)}) async-start(f32[2,16,2048]{2,1,0:T(8,128)} %broadcast_in_dim.21), calls=%async_computation | async-start | bytes 524288 | tf_op jit(solution)/shard_map/all_to_all | solution.py:12
  24.8 0.5 copy-start.10
  25.2 3.7 %copy-start.15 = (f32[96]{0:T(128)}, f32[96]{0:T(128)S(1)}, u32[]{:S(2)}) copy-start(f32[96]{0:T(128)S(1)} %fusion.13) | copy-start | bytes 1156
  69.2 1.9 %copy-start.3 = (bf16[1,2048,256]{2,1,0:T(8,128)(2,1)S(1)}, bf16[1,2048,256]{2,1,0:T(8,128)(2,1)}, u32[]{:S(2)}) copy-start(bf16[1,2048,256]{2,1,0:T(8,128)(2,1)} %param.34) | copy-start | bytes 3145732
  78.0 11.5 %copy-start.7 = (bf16[256,16]{0,1:T(8,128)(2,1)S(1)}, bf16[256,16]{0,1:T(8,128)(2,1)}, u32[]{:S(2)}) copy-start(bf16[256,16]{0,1:T(8,128)(2,1)} %param.39) | copy-start | bytes 24580
  78.0 37.5 %copy-start.11 = (s32[96]{0:T(128)S(1)}, s32[96]{0:T(128)}, u32[]{:S(2)}) copy-start(s32[96]{0:T(128)} %copy-done.10) | copy-start | bytes 1156
  78.0 37.5 %copy-start.16 = (f32[96]{0:T(128)S(1)}, f32[96]{0:T(128)}, u32[]{:S(2)}) copy-start(f32[96]{0:T(128)} %copy-done.15) | copy-start | bytes 1156
  85.8 34.8 %copy-start.12 = (bf16[2048,64]{0,1:T(8,128)(2,1)S(1)}, bf16[2048,64]{0,1:T(8,128)(2,1)}, u32[]{:S(2)}) copy-start(bf16[2048,64]{0,1:T(8,128)(2,1)} %param.28) | copy-start | bytes 786436
  85.8 29.7 %all-to-all-start.4 = ((bf16[8,4,4,1,2,1024]{5,4,2,1,3,0:T(2,128)(2,1)}), bf16[8,4,4,1,2,1024]{5,4,2,1,3,0:T(2,128)(2,1)S(1)}, u32[]{:S(2)}, u32[]{:S(2)}) async-start(bf16[8,4,4,1,2,1024]{5,4,2,1,3,0:T(2,128)(2,1)} %bitcast.79), calls=%async_computation.4 | async-start | bytes 1048576 | tf_op jit(solution)/shard_map/all_to_all | solution.py:47
  89.5 78.5 %all-gather.5.cloned.1.call-start = ((), (), s32[]{:S(2)}) async-start(), calls=%async_computation.9 | async-start | bytes 1179648 | tf_op jit(solution)/shard_map/all_gather | solution.py:68
  115.5 19.8 %copy-start.14 = (f32[2048]{0:T(1024)S(1)}, f32[2048]{0:T(1024)}, u32[]{:S(2)}) copy-start(f32[2048]{0:T(1024)} %param.40) | copy-start | bytes 24580
  116.8 18.7 %copy-start.13 = (bf16[2048,64]{0,1:T(8,128)(2,1)S(1)}, bf16[2048,64]{0,1:T(8,128)(2,1)}, u32[]{:S(2)}) copy-start(bf16[2048,64]{0,1:T(8,128)(2,1)} %param.27) | copy-start | bytes 786436
  116.8 11.7 %all-to-all-start.5 = ((bf16[8,4,4,1,2,1024]{5,4,2,0,3,1:T(2,128)(2,1)}), bf16[8,4,4,1,2,1024]{5,4,2,0,3,1:T(2,128)(2,1)S(1)}, u32[]{:S(2)}, u32[]{:S(2)}) async-start(bf16[8,4,4,1,2,1024]{5,4,2,0,3,1:T(2,128)(2,1)} %copy.70), calls=%async_computation.5 | async-start | bytes 1048576 | tf_op jit(solution)/shard_map/all_to_all | solution.py:47
  129.9 10.6 %all-to-all-start.6 = ((bf16[8,4,4,1,2,1024]{5,4,1,0,3,2:T(2,128)(2,1)}), bf16[8,4,4,1,2,1024]{5,4,1,0,3,2:T(2,128)(2,1)S(1)}, u32[]{:S(2)}, u32[]{:S(2)}) async-start(bf16[8,4,4,1,2,1024]{5,4,1,0,3,2:T(2,128)(2,1)} %copy.71), calls=%async_computation.6 | async-start | bytes 1048576 | tf_op jit(solution)/shard_map/all_to_all | solution.py:47
  146.2 4.4 %copy-start.9 = (f32[16,6]{0,1:T(8,128)S(1)}, f32[16,6]{0,1:T(8,128)}, u32[]{:S(2)}) copy-start(f32[16,6]{0,1:T(8,128)} %param.33) | copy-start | bytes 1156
  150.9 19.7 %copy-start.8 = (f32[2048]{0:T(1024)S(1)}, f32[2048]{0:T(1024)}, u32[]{:S(2)}) copy-start(f32[2048]{0:T(1024)} %param.41) | copy-start | bytes 24580
Sparse Core Ops, SparseCore 0:
  12.2 118.1 all-gather.2
  132.2 35.7 all-gather.4
where the time goes:
time: 179 us; the launch traced here: 178 us
  blocking collectives  73.6 us (41%)
  waiting for transfers between devices  27.4 us (15%)
  local copies, waits for them, and re-layouts  18.9 us (11%)
  matrix products  18.5 us (10%)
  starting transfers between devices  16.3 us (9%)
  between operations  14.5 us (8%)
  other arithmetic  9.14 us (5%)
    all_to_all x1, blocking collectives, shards(): lax.all_to_all(own_half, EP, split_axis=0, concat_axis=0, tiled=True)  33.7 us
    all_gather x2, blocking collectives, gathered_by_axis(): out = lax.all_gather(out, axes[number], axis=dim, tiled=True)  26 us
    all_gather x1, waiting for transfers between devices, gathered_by_axis(): out = lax.all_gather(out, axes[number], axis=dim, tiled=True)  15.5 us
    all_to_all x3, starting transfers between devices, moved_by_axis(): lax.all_to_all(tiles, axes[k], split_axis=k, concat_axis=k, tiled=True)  12.7 us
    all_to_all x3, waiting for transfers between devices, moved_by_axis(): lax.all_to_all(tiles, axes[k], split_axis=k, concat_axis=k, tiled=True)  11.2 us
    all_to_all x2, blocking collectives, sent_to_all(): return lax.all_to_all(copies, axis, split_axis=0, concat_axis=0, tiled=True)  9.15 us
    all_to_all x1, blocking collectives, sent_and_summed(): tiles = lax.all_to_all(split_up(value, dim, size), axis, 0, 0, tiled=True)  4.71 us
    transpose x2, local copies, waits for them, and re-layouts, in_order(): tiles = jnp.moveaxis(tiles, 0, dim)  4.22 us
  transfers between devices with their start and end apart: 6, of which 4 were waited for; matrix products, arithmetic and copies ran while one was open for 23% of the time, Pallas kernels for 0%

commit v1 on v0

v1 whole, which is shorter than its diff:
```python
import jax
import jax.numpy as jnp
from jax import lax
from jax.experimental import pallas as pl
from jax.experimental.pallas import tpu as pltpu
from jax.sharding import Mesh
from jax.sharding import PartitionSpec as P

EP = ("ep_0", "ep_1", "ep_2")
MESH = pl.DeviceIdType.MESH
BF = jnp.bfloat16
F32 = jnp.float32
NZ, NY, NX = 8, 4, 4
PLANE = NY * NX
ORDER = (0, 1, 7, 2, 6, 3, 5, 4)
SLOT = {d: i for i, d in enumerate(ORDER)}
OFFS = sorted(
    ((dy, dx) for dy in range(NY) for dx in range(NX) if (dy, dx) != (0, 0)),
    key=lambda o: min(o[0], NY - o[0]) + min(o[1], NX - o[1]),
)
BACK = [OFFS.index(((-dy) % NY, (-dx) % NX)) for dy, dx in OFFS]
NP = len(OFFS)


def dot(a, b):
    return jnp.dot(a, b, preferred_element_type=F32)


def dot_nt(a, b):
    return lax.dot_general(a, b, (((1,), (1,)), ((), ())), preferred_element_type=F32)


def dot_tn(a, b):
    return lax.dot_general(a, b, (((0,), (0,)), ((), ())), preferred_element_type=F32)


def rows(shape):
    return lax.broadcasted_iota(jnp.int32, shape, 0)


def cols(shape):
    return lax.broadcasted_iota(jnp.int32, shape, 1)


def ones_where(mask):
    return jnp.where(mask, 1.0, 0.0).astype(BF)


def norm(v, gain):
    center = jnp.mean(v, -1, keepdims=True)
    off = v - center
    spread = jnp.mean(off * off, -1, keepdims=True)
    return off * lax.rsqrt(spread + 1e-05) * gain


def halves(v):
    high = v.astype(BF)
    return high, (v - high.astype(F32)).astype(BF)


def body(
    tokens, norm_in, norm_mid, norm_out, mix_gate, routes, weights, dgate, dup, ddown,
    lens, bias, ck, cv, wq_h, wk_h, wv_h, wo_h, eg_h, eu_h, ed_h,
    out, fk, fv,
    kb, vb, wq, wk, wv, wo, eg, eu, ed,
    hb, pps, ppr, zb, ob, xb, yb, pbs, pbr, eb, rb, fs, fb, acc, fin,
    rts, rtb, dws, dwb, tb, d2s, d2b, das, dab, d4s, d4b, d4p,
    pm, wh, wl,
    lsem, zss, zrs, pss, prs, css, crs, pairs,
):
    z, y, x, c = (lax.axis_index(a) for a in (*EP, "tp"))
    me = y * NX + x
    o = 1 - c
    mate = (z, y, x, o)

    def along(d):
        return (lax.rem(z + d, NZ), y, x, c)

    def across(k):
        dy, dx = OFFS[k]
        return (z, lax.rem(y + dy, NY), lax.rem(x + dx, NX), c)

    def place(k):
        dy, dx = OFFS[k]
        return lax.rem(y + dy, NY) * NX + lax.rem(x + dx, NX)

    sent = []

    def send(src, dst, ss, rs, dev):
        copy = pltpu.make_async_remote_copy(
            src_ref=src, dst_ref=dst, send_sem=ss, recv_sem=rs, device_id=dev, device_id_type=MESH
        )
        copy.start()
        sent.append(copy)

    def got(dst, rs):
        pltpu.make_async_copy(dst, dst, rs).wait()

    def fetch(n, src, dst):
        copy = pltpu.make_async_copy(src, dst, lsem.at[n])
        copy.start()
        return copy

    l_wq = fetch(0, wq_h, wq)
    l_wk = fetch(1, wk_h, wk)
    l_wv = fetch(2, wv_h, wv)
    l_k = [fetch(3 + b, ck.at[b], kb.at[b]) for b in range(4)]
    l_v = [fetch(7 + b, cv.at[b], vb.at[b]) for b in range(4)]
    l_wo = fetch(11, wo_h, wo)
    l_eg = fetch(12, eg_h, eg)
    l_eu = fetch(13, eu_h, eu)
    l_ed = fetch(14, ed_h, ed)

    barrier = pltpu.get_barrier_semaphore()
    for d in range(1, NZ):
        pl.semaphore_signal(barrier, inc=1, device_id=along(d), device_id_type=MESH)
    for k in range(NP):
        pl.semaphore_signal(barrier, inc=1, device_id=across(k), device_id_type=MESH)
    pl.semaphore_signal(barrier, inc=1, device_id=mate, device_id_type=MESH)

    half = pl.ds(pl.multiple_of(c * 128, 128), 128)
    dws[0:16] = dgate[:, half]
    dws[16:32] = dup[:, half]
    dws[32:48] = ddown[:, half]
    rts[...] = jnp.zeros((16, 128), F32)
    for j in range(8):
        rts[0:6, 16 * j : 16 * j + 16] = routes[...].astype(F32)
        rts[8:14, 16 * j : 16 * j + 16] = weights[...]

    normed = norm(tokens[...].astype(F32), norm_in[...]).astype(BF)
    l_wq.wait()
    queries = dot(normed, wq[...]).astype(BF)
    l_wk.wait()
    fk[...] = dot_nt(normed, wk[...]).astype(BF)
    l_wv.wait()
    fv[...] = dot_nt(normed, wv[...]).astype(BF)

    pl.semaphore_wait(barrier, NZ - 1 + NP + 1)
    for k in range(NP):
        send(dws, dwb.at[me], pss.at[0, k], prs.at[0, BACK[k]], across(k))
    for d in ORDER[1:]:
        s = SLOT[NZ - d]
        send(rts, rtb.at[s], zss.at[0, SLOT[d]], zrs.at[0, s], along(d))
    dwb[me] = dws[...]
    rtb[0] = rts[...]

    wide = (64, 256)
    expand = ones_where(rows((64, 16)) // 4 == cols((64, 16)))
    fold = ones_where(lax.rem(rows((256, 256)), 64) == lax.rem(cols((256, 256)), 64))
    head_of = cols(wide) // 64 == lax.rem(rows(wide), 4)
    seq_of = cols(wide) // 64 == lax.rem(rows(wide) // 4, 4)
    picked = jnp.where(head_of, dot(expand, queries), 0.0).astype(BF)
    grid = jnp.where(seq_of, dot(picked, fold), 0.0).astype(BF)
    parts = []
    for b in range(4):
        l_k[b].wait()
        parts.append(dot(grid[16 * b : 16 * b + 16], kb[b]))
    scores = jnp.concatenate(parts, axis=0) * 0.125
    row = rows((64, 128))
    length = jnp.zeros((64, 128), jnp.int32)
    for s in range(16):
        length = jnp.where(row // 4 == s, lens[s], length)
    offset = jnp.zeros((64, 128), F32)
    for g in range(4):
        offset = jnp.where(lax.rem(row, 4) == g, bias[g], offset)
    later = ones_where(rows((128, 128)) >= cols((128, 128)))
    zs, keeps, seen = [], [], []
    for n in range(8):
        zn = scores[:, 128 * n : 128 * n + 128] + offset
        vis = cols((64, 128)) + 128 * n < length
        soft = jnp.maximum(zn, 0.0) + jnp.log1p(jnp.exp(-jnp.abs(zn)))
        zs.append(zn)
        seen.append(vis)
        keeps.append(jnp.where(vis, soft, 0.0))
    high, low = halves(jnp.concatenate(keeps, axis=0))
    within = dot(high, later) + dot(low, later)
    carry = jnp.zeros((64, 1), F32)
    sticks = [None] * 8
    for n in range(7, -1, -1):
        w = within[64 * n : 64 * n + 64]
        sticks[n] = jnp.where(seen[n], jnp.exp(zs[n] - w - carry), 0.0).astype(BF)
        carry = carry + w[:, 0:1]
    stick = jnp.concatenate(sticks, axis=1)
    parts = []
    for b in range(4):
        l_v[b].wait()
        parts.append(dot_nt(stick[16 * b : 16 * b + 16], vb[b]))
    att = jnp.where(seq_of, jnp.concatenate(parts, axis=0), 0.0).astype(BF)
    att = jnp.where(head_of, dot(att, fold), 0.0).astype(BF)
    gather = ones_where(cols((16, 64)) // 4 == rows((16, 64)))
    attended = dot(gather, att).astype(BF)
    l_wo.wait()
    pps[...] = dot(attended, wo[...])
    send(pps, ppr, css.at[0], crs.at[0], mate)

    for s in range(1, NZ):
        got(rtb.at[s], zrs.at[0, s])
    shape = (128, 64)
    expert = (z * PLANE + rows(shape) // 8).astype(F32)
    ahead = ones_where(
        (rows((64, 64)) < cols((64, 64))) & (rows((64, 64)) // 16 == cols((64, 64)) // 16)
    )
    for w in range(2):
        table = jnp.zeros((16, 64), F32)
        for j in range(4):
            table = jnp.where(cols((16, 64)) // 16 == j, rtb[4 * w + j][:, 0:64], table)
        hit = jnp.zeros(shape, F32)
        share = jnp.zeros(shape, F32)
        for k in range(6):
            same = table[k : k + 1] == expert
            hit = jnp.where(same, 1.0, hit)
            share = jnp.where(same, table[8 + k : 9 + k], share)
        rank = dot(hit.astype(BF), ahead)
        here = (
            (hit > 0.5)
            & (rank == lax.rem(rows(shape), 2).astype(F32))
            & (cols(shape) // 16 == lax.rem(rows(shape), 8) // 2)
        )
        pm[w] = ones_where(here)
        high, low = halves(jnp.where(here, share, 0.0))
        wh[w] = high
        wl[w] = low

    got(ppr, crs.at[0])
    hidden = norm(normed.astype(F32) + (pps[...] + ppr[...]), norm_mid[...]).astype(BF)
    hb[...] = hidden
    own_half = pl.ds(pl.multiple_of(c * 1024, 1024), 1024)
    mate_half = pl.ds(pl.multiple_of(o * 1024, 1024), 1024)
    for d in ORDER[1:]:
        s = SLOT[NZ - d]
        send(hb.at[:, own_half], zb.at[s], zss.at[1, SLOT[d]], zrs.at[1, s], along(d))
    zb[0] = hb[:, own_half]
    for d in ORDER[1:]:
        s = SLOT[NZ - d]
        there = pl.ds(pl.multiple_of(lax.rem(z + d, NZ) * 256, 256), 256)
        send(hb.at[:, there], tb.at[s], zss.at[2, SLOT[d]], zrs.at[2, s], along(d))
    tb[0] = hb[:, pl.ds(pl.multiple_of(z * 256, 256), 256)]
    mixing = jax.nn.sigmoid(jnp.sum(hidden.astype(F32) * mix_gate[...], -1, keepdims=True))

    def dispatch(w):
        for s in range(4 * w, 4 * w + 4):
            if s:
                got(zb.at[s], zrs.at[1, s])
        block = zb[4 * w : 4 * w + 4].reshape(64, 1024)
        going = dot(pm[w], block)
        for q in range(PLANE):
            ob[w, q] = going[8 * q : 8 * q + 8].astype(BF)
        for k in range(NP):
            send(
                ob.at[w, place(k)], xb.at[w, me], pss.at[1 + w, k], prs.at[1 + w, BACK[k]], across(k)
            )
        xb[w, me] = ob[w, me]
        send(ob.at[w, me], yb.at[w, me], css.at[1 + w], crs.at[1 + w], mate)

    def forward(w):
        for k in range(NP):
            slot = place(k)
            got(xb.at[w, slot], prs.at[1 + w, k])
            send(xb.at[w, slot], yb.at[w, slot], pairs.at[0, w, k], pairs.at[1, w, k], mate)

    def experts(w):
        got(yb.at[w, me], crs.at[1 + w])
        for k in range(NP):
            got(yb.at[w, place(k)], pairs.at[1, w, k])
        if w == 0:
            l_eg.wait()
            l_eu.wait()
        mine = xb[w].reshape(128, 1024)
        other = yb[w].reshape(128, 1024)
        gate = dot(mine, eg[own_half, :]) + dot(other, eg[mate_half, :])
        up = dot(mine, eu[own_half, :]) + dot(other, eu[mate_half, :])
        act = (jax.nn.silu(gate) * up).astype(BF)
        if w == 0:
            l_ed.wait()
        pbs[w] = dot(act, ed[:, mate_half]).astype(BF)
        send(pbs.at[w], pbr.at[w], css.at[3 + w], crs.at[3 + w], mate)
        return dot(act, ed[:, own_half]).astype(BF)

    def give_back(w, part):
        got(pbr.at[w], crs.at[3 + w])
        total = part.astype(F32) + pbr[w].astype(F32)
        for q in range(PLANE):
            eb[w, q] = total[8 * q : 8 * q + 8].astype(BF)
        for k in range(NP):
            send(
                eb.at[w, place(k)], rb.at[w, me], pss.at[3 + w, k], prs.at[3 + w, BACK[k]], across(k)
            )
        rb[w, me] = eb[w, me]

    def combine(w):
        for k in range(NP):
            got(rb.at[w, place(k)], prs.at[3 + w, k])
        block = rb[w].reshape(128, 1024)
        part = dot_tn(wh[w], block) + dot_tn(wl[w], block)
        for j in range(4):
            s = 4 * w + j
            piece = part[16 * j : 16 * j + 16]
            if s == 0:
                acc[...] = piece
            else:
                d = ORDER[s]
                t = SLOT[NZ - d]
                fs[s] = piece.astype(BF)
                send(fs.at[s], fb.at[t], zss.at[6, s], zrs.at[6, t], along(d))

    dispatch(0)

    for k in range(NP):
        got(dwb.at[place(k)], prs.at[0, k])
    for s in range(1, NZ):
        got(tb.at[s], zrs.at[2, s])
    column = tb[...].reshape(128, 256)
    pre = dot(column, dwb[:, 0:16, :].reshape(256, 128))
    lin = dot(column, dwb[:, 16:32, :].reshape(256, 128))
    for s in range(NZ):
        d2s[s, :, 0:128] = pre[16 * s : 16 * s + 16]
        d2s[s, :, 128:256] = lin[16 * s : 16 * s + 16]
    for d in ORDER[1:]:
        t = SLOT[NZ - d]
        send(d2s.at[SLOT[d]], d2b.at[t], zss.at[3, SLOT[d]], zrs.at[3, t], along(d))
    d2b[0] = d2s[0]

    dispatch(1)
    forward(0)
    part0 = experts(0)

    for s in range(1, NZ):
        got(d2b.at[s], zrs.at[3, s])
    total = jnp.sum(d2b[...], axis=0)
    das[...] = (jax.nn.silu(total[:, 0:128]) * total[:, 128:256]).astype(BF)
    for d in ORDER[1:]:
        t = SLOT[NZ - d]
        send(das, dab.at[t], zss.at[4, SLOT[d]], zrs.at[4, t], along(d))
    dab[0] = das[...]

    give_back(0, part0)
    forward(1)
    part1 = experts(1)

    for s in range(1, NZ):
        got(dab.at[s], zrs.at[4, s])
    cols_out = dot_nt(dab[...].reshape(128, 128), dwb[:, 32:48, :].reshape(256, 128))
    for s in range(NZ):
        d4s[s] = cols_out[16 * s : 16 * s + 16]
    for d in ORDER[1:]:
        send(d4s.at[SLOT[d]], d4b.at[z], zss.at[5, SLOT[d]], zrs.at[5, SLOT[NZ - d]], along(d))
    d4b[z] = d4s[0]

    give_back(1, part1)
    combine(0)

    for d in ORDER[1:]:
        got(d4b.at[lax.rem(z + d, NZ)], zrs.at[5, SLOT[d]])
    send(d4b, d4p, css.at[5], crs.at[5], mate)

    combine(1)
    got(d4p, crs.at[5])
    mixed = hidden.astype(F32) + mixing * jnp.concatenate(
        [d4b[n] + d4p[n] for n in range(NZ)], axis=1
    )
    total = acc[...]
    for s in range(1, NZ):
        got(fb.at[s], zrs.at[6, s])
        total = total + fb[s].astype(F32)
    fin[:, own_half] = total
    send(fin.at[:, own_half], fin.at[:, own_half], css.at[6], crs.at[6], mate)
    got(fin.at[:, mate_half], crs.at[6])
    out[...] = norm(mixed + fin[...], norm_out[...]).astype(BF)

    for copy in sent:
        copy.wait_send()


def shards(
    tokens, cache_keys, cache_values, cache_lengths, norm_in, w_query, w_key, w_value,
    stick_bias, w_output, norm_mid, routes, route_weights, expert_gate, expert_up,
    expert_down, dense_gate, dense_up, dense_down, mix_gate, norm_out,
):
    vmem = pl.BlockSpec(memory_space=pltpu.VMEM)
    smem = pl.BlockSpec(memory_space=pltpu.SMEM)
    hbm = pl.BlockSpec(memory_space=pl.ANY)
    dma = pltpu.SemaphoreType.DMA
    V = pltpu.VMEM
    return pl.pallas_call(
        body,
        out_shape=(
            jax.ShapeDtypeStruct((16, 2048), BF),
            jax.ShapeDtypeStruct((16, 64), BF),
            jax.ShapeDtypeStruct((16, 64), BF),
        ),
        in_specs=[vmem] * 10 + [smem] * 2 + [hbm] * 9,
        out_specs=(vmem, vmem, vmem),
        scratch_shapes=[
            V((4, 256, 1024), BF),
            V((4, 256, 1024), BF),
            V((2048, 256), BF),
            V((64, 2048), BF),
            V((64, 2048), BF),
            V((256, 2048), BF),
            V((2048, 256), BF),
            V((2048, 256), BF),
            V((256, 2048), BF),
            V((16, 2048), BF),
            V((16, 2048), F32),
            V((16, 2048), F32),
            V((8, 16, 1024), BF),
            V((2, 16, 8, 1024), BF),
            V((2, 16, 8, 1024), BF),
            V((2, 16, 8, 1024), BF),
            V((2, 128, 1024), BF),
            V((2, 128, 1024), BF),
            V((2, 16, 8, 1024), BF),
            V((2, 16, 8, 1024), BF),
            V((8, 16, 1024), BF),
            V((8, 16, 1024), BF),
            V((16, 1024), F32),
            V((16, 2048), F32),
            V((16, 128), F32),
            V((8, 16, 128), F32),
            V((48, 128), BF),
            V((16, 48, 128), BF),
            V((8, 16, 256), BF),
            V((8, 16, 256), F32),
            V((8, 16, 256), F32),
            V((16, 128), BF),
            V((8, 16, 128), BF),
            V((8, 16, 256), F32),
            V((8, 16, 256), F32),
            V((8, 16, 256), F32),
            V((2, 128, 64), BF),
            V((2, 128, 64), BF),
            V((2, 128, 64), BF),
            dma((15,)),
            dma((7, 8)),
            dma((7, 8)),
            dma((5, 15)),
            dma((5, 15)),
            dma((7,)),
            dma((7,)),
            dma((2, 2, 15)),
        ],
        compiler_params=pltpu.CompilerParams(
            collective_id=0, has_side_effects=True, vmem_limit_bytes=67043328
        ),
    )(
        tokens,
        norm_in.reshape(1, -1),
        norm_mid.reshape(1, -1),
        norm_out.reshape(1, -1),
        mix_gate.reshape(1, -1),
        routes.T,
        route_weights.T,
        dense_gate,
        dense_up,
        dense_down.T,
        cache_lengths,
        stick_bias,
        cache_keys.reshape(4, 256, 1024),
        cache_values.reshape(4, 256, 1024),
        w_query,
        w_key.T,
        w_value.T,
        w_output,
        expert_gate.reshape(2048, 256),
        expert_up.reshape(2048, 256),
        expert_down.reshape(256, 2048),
    )


def solution(mesh):
    split = Mesh(
        mesh.devices.reshape(NZ, NY, NX, mesh.shape["tp"]), ("ep_0", "ep_1", "ep_2", "tp")
    )
    return jax.shard_map(
        shards,
        mesh=split,
        in_specs=(
            P(EP, None),
            P(EP, "tp", None, None),
            P(EP, "tp", None, None),
            P(EP),
            P(),
            P(None, "tp"),
            P(None, "tp"),
            P(None, "tp"),
            P("tp"),
            P("tp", None),
            P(),
            P(EP, None),
            P(EP, None),
            P(EP, None, "tp"),
            P(EP, None, "tp"),
            P(EP, "tp", None),
            P(EP, None),
            P(EP, None),
            P(None, EP),
            P(),
            P(),
        ),
        out_specs=(P(EP, None), P(EP, "tp"), P(EP, "tp")),
        check_vma=False,
    )
```

time: 179 us -> 62.4 us (0.35)
  the two profiles are of different devices: /device:TPU:4 before, /device:TPU:1 now
where the time goes in v1:
time: 62.4 us; the launch traced here: 62.1 us
  Pallas kernels  57.5 us (92%)
  local copies, waits for them, and re-layouts  4.02 us (6%)
  between operations  0.65 us (1%)
    pallas_call x1, Pallas kernels, shards(): pl.pallas_call(body, out_shape=(jax.ShapeDtypeStruct((16, 2048), BF), jax...  57.5 us
    unnamed x3, local copies, waits for them, and re-layouts  4.02 us

profile of v1, /device:TPU:1, one launch (start us, length us, event | category | flops | bytes accessed | tf_op | source)
XLA Modules:
  0.0 62.1 jit_solution(2908908572507685130)
XLA Ops:
  0.6 57.5 %shard_map.220 = (bf16[16,2048]{1,0:T(8,128)(2,1)}, bf16[16,64]{1,0:T(8,128)(2,1)}, bf16[16,64]{1,0:T(8,128)(2,1)}) custom-call(bf16[16,2048]{1,0:T(8,128)(2,1)} %tokens.1, f32[1,2048]{1,0:T(1,128)} %bitcast.21, f32[1,2048]{1,0:T(1,128)} %bitcast.22, f32[1,2048]{1,0:T(1,128)} %bitcast.23, f32[1,2048]{1,0:T(1,128)} %bitcast.24, s32[6,16]{1,0:T(8,128)} %bitcast.26, ...), custom_call_target="tpu_custom_call" | custom-call | tf_op jit(solution)/shard_map/pallas_call | solution.py:384
  58.1 1.5 %copy.27 = bf16[16,2048]{1,0:T(8,128)(2,1)} copy(bf16[16,2048]{1,0:T(8,128)(2,1)} %get-tuple-element.6) | data formatting | bytes 131072
  59.6 1.3 %copy.28 = bf16[16,64]{1,0:T(8,128)(2,1)} copy(bf16[16,64]{1,0:T(8,128)(2,1)} %get-tuple-element.7) | data formatting | bytes 4096
  60.9 1.3 %copy.29 = bf16[16,64]{1,0:T(8,128)(2,1)} copy(bf16[16,64]{1,0:T(8,128)(2,1)} %get-tuple-element.8) | data formatting | bytes 4096

commit v2 on v1

v2 whole, which is shorter than its diff:
```python
import jax
import jax.numpy as jnp
from jax import lax
from jax.experimental import pallas as pl
from jax.experimental.pallas import tpu as pltpu
from jax.sharding import Mesh
from jax.sharding import PartitionSpec as P

EP = ("ep_0", "ep_1", "ep_2")
MESH = pl.DeviceIdType.MESH
BF = jnp.bfloat16
F32 = jnp.float32
NZ, NY, NX = 8, 4, 4
PLANE = NY * NX
ORDER = (0, 4, 1, 7, 2, 6, 3, 5)
SLOT = {d: i for i, d in enumerate(ORDER)}
OFFS = sorted(
    ((dy, dx) for dy in range(NY) for dx in range(NX) if (dy, dx) != (0, 0)),
    key=lambda o: min(o[0], NY - o[0]) + min(o[1], NX - o[1]),
)
BACK = [OFFS.index(((-dy) % NY, (-dx) % NX)) for dy, dx in OFFS]
NP = len(OFFS)


def dot(a, b):
    return jnp.dot(a, b, preferred_element_type=F32)


def dot_nt(a, b):
    return lax.dot_general(a, b, (((1,), (1,)), ((), ())), preferred_element_type=F32)


def rows(shape):
    return lax.broadcasted_iota(jnp.int32, shape, 0)


def cols(shape):
    return lax.broadcasted_iota(jnp.int32, shape, 1)


def ones_where(mask):
    return jnp.where(mask, 1.0, 0.0).astype(BF)


def norm(v, gain):
    center = jnp.mean(v, -1, keepdims=True)
    off = v - center
    spread = jnp.mean(off * off, -1, keepdims=True)
    return off * lax.rsqrt(spread + 1e-05) * gain


def halves(v):
    high = v.astype(BF)
    return high, (v - high.astype(F32)).astype(BF)


def body(
    tokens_h, norm_in_h, wq_h, wk_h, wv_h, lens_h, bias_h, ck, cv, dgate_h, dup_h, ddown_h,
    routes_h, weights_h, wo_h, norm_mid_h, mix_gate_h, eg_h, eu_h, ed_h, norm_out_h,
    out, fk, fv,
    tokens, norm_in, wq, wk, wv, lens, bias, kb, vb, dgate, dup, ddown,
    routes, weights, wo, norm_mid, mix_gate, eg, eu, ed, norm_out,
    hb, pps, ppr, zb, ob, xb, yb, pbs, pbr, eb, rb, fs, fb, acc, fin,
    rts, rtb, dws, dwb, tb, d2s, d2b, das, dab, d4s, d4b, d4p,
    pm, wh, wl,
    lsem, bank,
):
    z, y, x, c = (lax.axis_index(a) for a in (*EP, "tp"))
    me = y * NX + x
    o = 1 - c
    mate = (z, y, x, o)

    def along(d):
        return (lax.rem(z + d, NZ), y, x, c)

    def across(k):
        dy, dx = OFFS[k]
        return (z, lax.rem(y + dy, NY), lax.rem(x + dx, NX), c)

    def place(k):
        dy, dx = OFFS[k]
        return lax.rem(y + dy, NY) * NX + lax.rem(x + dx, NX)

    flags = {}

    def flag(*name):
        return bank.at[flags.setdefault(name, len(flags))]

    def send(src, dst, out_flag, in_flag, dev):
        pltpu.make_async_remote_copy(
            src_ref=src, dst_ref=dst, send_sem=out_flag, recv_sem=in_flag,
            device_id=dev, device_id_type=MESH,
        ).start()

    def await_bytes(ref, name):
        pltpu.make_async_copy(ref, ref, name).wait()

    reads = {}

    def fetch(name, src, dst):
        copy = pltpu.make_async_copy(src, dst, lsem.at[len(reads)])
        copy.start()
        reads[name] = copy

    def ready(*names):
        for name in names:
            reads[name].wait()

    fetch("tokens", tokens_h, tokens)
    fetch("norm_in", norm_in_h, norm_in)
    fetch("wq", wq_h, wq)
    fetch("wk", wk_h, wk)
    fetch("wv", wv_h, wv)
    fetch("dgate", dgate_h, dgate)
    fetch("dup", dup_h, dup)
    fetch("ddown", ddown_h, ddown)
    fetch("routes", routes_h, routes)
    fetch("weights", weights_h, weights)
    for b in range(4):
        fetch(("k", b), ck.at[b], kb.at[b])
    fetch("lens", lens_h, lens)
    fetch("bias", bias_h, bias)
    for b in range(4):
        fetch(("v", b), cv.at[b], vb.at[b])
    fetch("wo", wo_h, wo)
    fetch("norm_mid", norm_mid_h, norm_mid)
    fetch("mix_gate", mix_gate_h, mix_gate)
    fetch("eg", eg_h, eg)
    fetch("eu", eu_h, eu)
    fetch("ed", ed_h, ed)
    fetch("norm_out", norm_out_h, norm_out)

    barrier = pltpu.get_barrier_semaphore()
    for d in range(1, NZ):
        pl.semaphore_signal(barrier, inc=1, device_id=along(d), device_id_type=MESH)
    for k in range(NP):
        pl.semaphore_signal(barrier, inc=1, device_id=across(k), device_id_type=MESH)
    pl.semaphore_signal(barrier, inc=1, device_id=mate, device_id_type=MESH)

    ready("tokens", "norm_in")
    normed = norm(tokens[...].astype(F32), norm_in[...]).astype(BF)
    ready("wq")
    queries = dot(normed, wq[...]).astype(BF)
    ready("wk")
    fk[...] = dot_nt(normed, wk[...]).astype(BF)
    ready("wv")
    fv[...] = dot_nt(normed, wv[...]).astype(BF)

    half = pl.ds(pl.multiple_of(c * 128, 128), 128)
    ready("dgate", "dup", "ddown", "routes", "weights")
    dws[0:16] = dgate[:, half]
    dws[16:32] = dup[:, half]
    dws[32:48] = ddown[:, half]
    rts[...] = jnp.zeros((16, 128), F32)
    for j in range(8):
        rts[0:6, 16 * j : 16 * j + 16] = routes[...].astype(F32)
        rts[8:14, 16 * j : 16 * j + 16] = weights[...]

    pl.semaphore_wait(barrier, NZ - 1 + NP + 1)
    for k in range(NP):
        send(dws, dwb.at[me], flag("ws"), flag("wr"), across(k))
    for d in ORDER[1:]:
        send(rts, rtb.at[SLOT[NZ - d]], flag("ts"), flag("tr"), along(d))
    dwb[me] = dws[...]
    rtb[0] = rts[...]

    wide = (64, 256)
    expand = ones_where(rows((64, 16)) // 4 == cols((64, 16)))
    fold = ones_where(lax.rem(rows((256, 256)), 64) == lax.rem(cols((256, 256)), 64))
    head_of = cols(wide) // 64 == lax.rem(rows(wide), 4)
    seq_of = cols(wide) // 64 == lax.rem(rows(wide) // 4, 4)
    picked = jnp.where(head_of, dot(expand, queries), 0.0).astype(BF)
    grid = jnp.where(seq_of, dot(picked, fold), 0.0).astype(BF)
    parts = []
    for b in range(4):
        ready(("k", b))
        parts.append(dot(grid[16 * b : 16 * b + 16], kb[b]))
    scores = jnp.concatenate(parts, axis=0) * 0.125
    ready("lens", "bias")
    row = rows((64, 128))
    length = jnp.zeros((64, 128), jnp.int32)
    for s in range(16):
        length = jnp.where(row // 4 == s, lens[s], length)
    offset = jnp.zeros((64, 128), F32)
    for g in range(4):
        offset = jnp.where(lax.rem(row, 4) == g, bias[g], offset)
    later = ones_where(rows((128, 128)) >= cols((128, 128)))
    zs, keeps, seen = [], [], []
    for n in range(8):
        zn = scores[:, 128 * n : 128 * n + 128] + offset
        vis = cols((64, 128)) + 128 * n < length
        soft = jnp.maximum(zn, 0.0) + jnp.log1p(jnp.exp(-jnp.abs(zn)))
        zs.append(zn)
        seen.append(vis)
        keeps.append(jnp.where(vis, soft, 0.0))
    high, low = halves(jnp.concatenate(keeps, axis=0))
    within = dot(high, later) + dot(low, later)
    carry = jnp.zeros((64, 1), F32)
    sticks = [None] * 8
    for n in range(7, -1, -1):
        w = within[64 * n : 64 * n + 64]
        sticks[n] = jnp.where(seen[n], jnp.exp(zs[n] - w - carry), 0.0).astype(BF)
        carry = carry + w[:, 0:1]
    stick = jnp.concatenate(sticks, axis=1)
    parts = []
    for b in range(4):
        ready(("v", b))
        parts.append(dot_nt(stick[16 * b : 16 * b + 16], vb[b]))
    att = jnp.where(seq_of, jnp.concatenate(parts, axis=0), 0.0).astype(BF)
    att = jnp.where(head_of, dot(att, fold), 0.0).astype(BF)
    gather = ones_where(cols((16, 64)) // 4 == rows((16, 64)))
    attended = dot(gather, att).astype(BF)
    ready("wo")
    pps[...] = dot(attended, wo[...])
    send(pps, ppr, flag("ps"), flag("pr"), mate)

    await_bytes(rtb.at[1:8], flag("tr"))
    shape = (128, 64)
    expert = (z * PLANE + rows(shape) // 8).astype(F32)
    ahead = ones_where(
        (rows((64, 64)) < cols((64, 64))) & (rows((64, 64)) // 16 == cols((64, 64)) // 16)
    )
    for w in range(2):
        table = jnp.zeros((16, 64), F32)
        for j in range(4):
            table = jnp.where(cols((16, 64)) // 16 == j, rtb[4 * w + j][:, 0:64], table)
        hit = jnp.zeros(shape, F32)
        share = jnp.zeros(shape, F32)
        for k in range(6):
            same = table[k : k + 1] == expert
            hit = jnp.where(same, 1.0, hit)
            share = jnp.where(same, table[8 + k : 9 + k], share)
        rank = dot(hit.astype(BF), ahead)
        here = (
            (hit > 0.5)
            & (rank == lax.rem(rows(shape), 2).astype(F32))
            & (cols(shape) // 16 == lax.rem(rows(shape), 8) // 2)
        )
        pm[w] = ones_where(here)
        high, low = halves(jnp.transpose(jnp.where(here, share, 0.0)))
        wh[w] = high
        wl[w] = low
    await_bytes(rtb.at[1:8], flag("ts"))
    await_bytes(dwb.at[0:15], flag("ws"))

    own_half = pl.ds(pl.multiple_of(c * 1024, 1024), 1024)
    mate_half = pl.ds(pl.multiple_of(o * 1024, 1024), 1024)
    ready("norm_mid", "mix_gate")
    await_bytes(ppr, flag("pr"))
    hidden = norm(normed.astype(F32) + (pps[...] + ppr[...]), norm_mid[...]).astype(BF)
    hb[...] = hidden
    for d in (4, 1, 7, 3, 5, 2, 6):
        t = SLOT[NZ - d]
        send(hb.at[:, own_half], zb.at[t], flag("zs"), flag("zr", t // 4), along(d))
    zb[0] = hb[:, own_half]
    mixing = jax.nn.sigmoid(jnp.sum(hidden.astype(F32) * mix_gate[...], -1, keepdims=True))
    await_bytes(pps, flag("ps"))

    def dispatch(w):
        await_bytes(zb.at[1:4] if w == 0 else zb.at[4:8], flag("zr", w))
        block = zb[4 * w : 4 * w + 4].reshape(64, 1024)
        going = dot(pm[w], block)
        for q in range(PLANE):
            ob[w, q] = going[8 * q : 8 * q + 8].astype(BF)
        for k in range(NP):
            send(
                ob.at[w, place(k)], xb.at[w, me], flag("xs", w), flag("xr", w, BACK[k]), across(k)
            )
        send(ob.at[w, me], yb.at[w, me], flag("ys", w), flag("yr", w), mate)
        xb[w, me] = ob[w, me]

    def forward(w):
        for k in range(NP):
            slot = place(k)
            await_bytes(xb.at[w, slot], flag("xr", w, k))
            send(xb.at[w, slot], yb.at[w, slot], flag("ys", w), flag("yr", w), mate)

    def experts(w):
        if w == 0:
            ready("eg", "eu", "ed")
        mine = xb[w].reshape(128, 1024)
        gate = dot(mine, eg[own_half, :])
        up = dot(mine, eu[own_half, :])
        await_bytes(xb.at[w, 0:15], flag("xs", w))
        await_bytes(yb.at[w], flag("yr", w))
        other = yb[w].reshape(128, 1024)
        gate = gate + dot(other, eg[mate_half, :])
        up = up + dot(other, eu[mate_half, :])
        act = (jax.nn.silu(gate) * up).astype(BF)
        pbs[w] = dot(act, ed[:, mate_half]).astype(BF)
        send(pbs.at[w], pbr.at[w], flag("bs", w), flag("br", w), mate)
        part = dot(act, ed[:, own_half]).astype(BF)
        await_bytes(yb.at[w], flag("ys", w))
        return part

    def give_back(w, part):
        await_bytes(pbr.at[w], flag("br", w))
        total = part.astype(F32) + pbr[w].astype(F32)
        for q in range(PLANE):
            eb[w, q] = total[8 * q : 8 * q + 8].astype(BF)
        for k in range(NP):
            send(eb.at[w, place(k)], rb.at[w, me], flag("es", w), flag("er", w), across(k))
        rb[w, me] = eb[w, me]
        await_bytes(pbr.at[w], flag("bs", w))

    def combine(w):
        await_bytes(rb.at[w, 0:15], flag("er", w))
        block = rb[w].reshape(128, 1024)
        part = dot(wh[w], block) + dot(wl[w], block)
        for j in range(4):
            s = 4 * w + j
            piece = part[16 * j : 16 * j + 16]
            if s == 0:
                acc[...] = piece
            else:
                d = ORDER[s]
                fs[s] = piece.astype(BF)
                send(fs.at[s], fb.at[SLOT[NZ - d]], flag("fs", w), flag("fr", w), along(d))
        await_bytes(rb.at[w, 0:15], flag("es", w))

    dispatch(0)
    dispatch(1)

    holder = c == z // 4
    features = pl.ds(pl.multiple_of(lax.rem(z, 4) * 256, 256), 256)

    @pl.when(holder)
    def _():
        send(zb.at[:, :, features], tb, flag("cs"), flag("cr"), mate)
        tb[...] = zb[:, :, features]
        await_bytes(tb, flag("cs"))

    await_bytes(dwb.at[0:15], flag("wr"))

    @pl.when(jnp.logical_not(holder))
    def _():
        await_bytes(tb, flag("cr"))

    column = tb[...].reshape(128, 256)
    pre = dot(column, dwb[:, 0:16, :].reshape(256, 128))
    lin = dot(column, dwb[:, 16:32, :].reshape(256, 128))
    for s in range(NZ):
        d2s[s, :, 0:128] = pre[16 * s : 16 * s + 16]
        d2s[s, :, 128:256] = lin[16 * s : 16 * s + 16]
    for d in ORDER[1:]:
        send(d2s.at[SLOT[d]], d2b.at[SLOT[NZ - d]], flag("d2s"), flag("d2r"), along(d))
    d2b[0] = d2s[0]

    forward(0)
    part0 = experts(0)
    give_back(0, part0)
    await_bytes(zb.at[1:8], flag("zs"))
    forward(1)
    part1 = experts(1)

    await_bytes(d2b.at[1:8], flag("d2r"))
    total = jnp.sum(d2b[...], axis=0)
    das[...] = (jax.nn.silu(total[:, 0:128]) * total[:, 128:256]).astype(BF)
    for d in ORDER[1:]:
        send(das, dab.at[SLOT[NZ - d]], flag("d3s"), flag("d3r"), along(d))
    dab[0] = das[...]

    give_back(1, part1)
    combine(0)

    await_bytes(d2b.at[1:8], flag("d2s"))
    await_bytes(dab.at[1:8], flag("d3r"))
    cols_out = dot_nt(dab[...].reshape(128, 128), dwb[:, 32:48, :].reshape(256, 128))
    for s in range(NZ):
        d4s[s] = cols_out[16 * s : 16 * s + 16]
    for d in ORDER[1:]:
        send(d4s.at[SLOT[d]], d4b.at[z], flag("d4s"), flag("d4r"), along(d))
    d4b[z] = d4s[0]
    await_bytes(dab.at[1:8], flag("d3s"))

    combine(1)
    await_bytes(d4b.at[0:7], flag("d4r"))
    send(d4b, d4p, flag("d5s"), flag("d5r"), mate)
    ready("norm_out")
    await_bytes(fb.at[1:4], flag("fr", 0))
    total = acc[...] + fb[1].astype(F32) + fb[2].astype(F32) + fb[3].astype(F32)
    await_bytes(d4p, flag("d5r"))
    mixed = hidden.astype(F32) + mixing * jnp.concatenate(
        [d4b[n] + d4p[n] for n in range(NZ)], axis=1
    )
    await_bytes(d4b.at[0:7], flag("d4s"))
    await_bytes(d4p, flag("d5s"))
    await_bytes(fb.at[1:4], flag("fs", 0))
    await_bytes(fb.at[4:8], flag("fr", 1))
    for s in range(4, NZ):
        total = total + fb[s].astype(F32)
    fin[:, own_half] = total
    send(fin.at[:, own_half], fin.at[:, own_half], flag("us"), flag("ur"), mate)
    await_bytes(fb.at[4:8], flag("fs", 1))
    await_bytes(fin.at[:, mate_half], flag("ur"))
    out[...] = norm(mixed + fin[...], norm_out[...]).astype(BF)
    await_bytes(fin.at[:, own_half], flag("us"))


def shards(
    tokens, cache_keys, cache_values, cache_lengths, norm_in, w_query, w_key, w_value,
    stick_bias, w_output, norm_mid, routes, route_weights, expert_gate, expert_up,
    expert_down, dense_gate, dense_up, dense_down, mix_gate, norm_out,
):
    vmem = pl.BlockSpec(memory_space=pltpu.VMEM)
    hbm = pl.BlockSpec(memory_space=pltpu.HBM)
    dma = pltpu.SemaphoreType.DMA
    V = pltpu.VMEM
    return pl.pallas_call(
        body,
        out_shape=(V((16, 2048), BF), V((16, 64), BF), V((16, 64), BF)),
        in_specs=[hbm] * 21,
        out_specs=(vmem, vmem, vmem),
        scratch_shapes=[
            V((16, 2048), BF),
            V((1, 2048), F32),
            V((2048, 256), BF),
            V((64, 2048), BF),
            V((64, 2048), BF),
            pltpu.SMEM((16,), jnp.int32),
            pltpu.SMEM((4,), F32),
            V((4, 256, 1024), BF),
            V((4, 256, 1024), BF),
            V((16, 256), BF),
            V((16, 256), BF),
            V((16, 256), BF),
            V((6, 16), jnp.int32),
            V((6, 16), F32),
            V((256, 2048), BF),
            V((1, 2048), F32),
            V((1, 2048), F32),
            V((2048, 256), BF),
            V((2048, 256), BF),
            V((256, 2048), BF),
            V((1, 2048), F32),
            V((16, 2048), BF),
            V((16, 2048), F32),
            V((16, 2048), F32),
            V((8, 16, 1024), BF),
            V((2, 16, 8, 1024), BF),
            V((2, 16, 8, 1024), BF),
            V((2, 16, 8, 1024), BF),
            V((2, 128, 1024), BF),
            V((2, 128, 1024), BF),
            V((2, 16, 8, 1024), BF),
            V((2, 16, 8, 1024), BF),
            V((8, 16, 1024), BF),
            V((8, 16, 1024), BF),
            V((16, 1024), F32),
            V((16, 2048), F32),
            V((16, 128), F32),
            V((8, 16, 128), F32),
            V((48, 128), BF),
            V((16, 48, 128), BF),
            V((8, 16, 256), BF),
            V((8, 16, 256), F32),
            V((8, 16, 256), F32),
            V((16, 128), BF),
            V((8, 16, 128), BF),
            V((8, 16, 256), F32),
            V((8, 16, 256), F32),
            V((8, 16, 256), F32),
            V((2, 128, 64), BF),
            V((2, 64, 128), BF),
            V((2, 64, 128), BF),
            dma((27,)),
            dma((96,)),
        ],
        compiler_params=pltpu.CompilerParams(
            collective_id=0, has_side_effects=True, vmem_limit_bytes=56 * 1024 * 1024
        ),
    )(
        tokens,
        norm_in.reshape(1, -1),
        w_query,
        w_key.T,
        w_value.T,
        cache_lengths,
        stick_bias,
        cache_keys.reshape(4, 256, 1024),
        cache_values.reshape(4, 256, 1024),
        dense_gate,
        dense_up,
        dense_down.T,
        routes.T,
        route_weights.T,
        w_output,
        norm_mid.reshape(1, -1),
        mix_gate.reshape(1, -1),
        expert_gate.reshape(2048, 256),
        expert_up.reshape(2048, 256),
        expert_down.reshape(256, 2048),
        norm_out.reshape(1, -1),
    )


def solution(mesh):
    split = Mesh(
        mesh.devices.reshape(NZ, NY, NX, mesh.shape["tp"]), ("ep_0", "ep_1", "ep_2", "tp")
    )
    return jax.shard_map(
        shards,
        mesh=split,
        in_specs=(
            P(EP, None),
            P(EP, "tp", None, None),
            P(EP, "tp", None, None),
            P(EP),
            P(),
            P(None, "tp"),
            P(None, "tp"),
            P(None, "tp"),
            P("tp"),
            P("tp", None),
            P(),
            P(EP, None),
            P(EP, None),
            P(EP, None, "tp"),
            P(EP, None, "tp"),
            P(EP, "tp", None),
            P(EP, None),
            P(EP, None),
            P(None, EP),
            P(),
            P(),
        ),
        out_specs=(P(EP, None), P(EP, "tp"), P(EP, "tp")),
        check_vma=False,
    )
```

time: 62.4 us -> 54.1 us (0.87)
  Pallas kernels: 57.5 us -> 51.6 us
  local copies, waits for them, and re-layouts: 4.02 us -> 1.82 us
    pallas_call x1, Pallas kernels: 57.5 us -> 51.6 us  [shards(): pl.pallas_call(body, out_shape=(V((16, 2048), BF), V((16, 64), BF), V((16...]
    unnamed x3, local copies, waits for them, and re-layouts: 4.02 us -> 1.82 us
where the time goes in v2:
time: 54.1 us; the launch traced here: 54 us
  Pallas kernels  51.6 us (95%)
  local copies, waits for them, and re-layouts  1.82 us (3%)
  between operations  0.65 us (1%)
    pallas_call x1, Pallas kernels, shards(): pl.pallas_call(body, out_shape=(V((16, 2048), BF), V((16, 64), BF), V((16...  51.6 us
    unnamed x3, local copies, waits for them, and re-layouts  1.82 us

profile of v2, /device:TPU:1, one launch (start us, length us, event | category | flops | bytes accessed | tf_op | source)
XLA Modules:
  0.0 54.0 jit_solution(12810027079156014124)
XLA Ops:
  0.6 51.6 %shard_map.220 = (bf16[16,2048]{1,0:T(8,128)(2,1)S(1)}, bf16[16,64]{1,0:T(8,128)(2,1)S(1)}, bf16[16,64]{1,0:T(8,128)(2,1)S(1)}) custom-call(bf16[16,2048]{1,0:T(8,128)(2,1)} %tokens_h.1, f32[1,2048]{1,0:T(1,128)} %bitcast.21, bf16[2048,256]{1,0:T(8,128)(2,1)} %wq_h.1, bf16[64,2048]{1,0:T(8,128)(2,1)} %bitcast.19, bf16[64,2048]{1,0:T(8,128)(2,1)} %bitcast.20, ...), custom_call_target="tpu_custom_call" | custom-call | tf_op jit(solution)/shard_map/pallas_call | solution.py:409
  52.2 0.6 %copy.27 = bf16[16,2048]{1,0:T(8,128)(2,1)} copy(bf16[16,2048]{1,0:T(8,128)(2,1)S(1)} %get-tuple-element.3) | data formatting | bytes 131072
  52.8 0.6 %copy.28 = bf16[16,64]{1,0:T(8,128)(2,1)} copy(bf16[16,64]{1,0:T(8,128)(2,1)S(1)} %get-tuple-element.4) | data formatting | bytes 4096
  53.4 0.6 %copy.29 = bf16[16,64]{1,0:T(8,128)(2,1)} copy(bf16[16,64]{1,0:T(8,128)(2,1)S(1)} %get-tuple-element.5) | data formatting | bytes 4096

commit v3 on v2

--- a/solution.py
+++ b/solution.py
@@ -20,6 +20,8 @@
 )
 BACK = [OFFS.index(((-dy) % NY, (-dx) % NX)) for dy, dx in OFFS]
 NP = len(OFFS)
+NC = 4
+HW = 1024 // NC
 
 
 def dot(a, b):
@@ -60,9 +62,9 @@
     out, fk, fv,
     tokens, norm_in, wq, wk, wv, lens, bias, kb, vb, dgate, dup, ddown,
     routes, weights, wo, norm_mid, mix_gate, eg, eu, ed, norm_out,
-    hb, pps, ppr, zb, ob, xb, yb, pbs, pbr, eb, rb, fs, fb, acc, fin,
+    egm, eum, edm, hb, pps, ppr, zb, ob, xb, eb, rb, fs, fb, fin,
     rts, rtb, dws, dwb, tb, d2s, d2b, das, dab, d4s, d4b, d4p,
-    pm, wh, wl,
+    pm, wh, wl, ga,
     lsem, bank,
 ):
     z, y, x, c = (lax.axis_index(a) for a in (*EP, "tp"))
@@ -125,10 +127,6 @@
     fetch("wo", wo_h, wo)
     fetch("norm_mid", norm_mid_h, norm_mid)
     fetch("mix_gate", mix_gate_h, mix_gate)
-    fetch("eg", eg_h, eg)
-    fetch("eu", eu_h, eu)
-    fetch("ed", ed_h, ed)
-    fetch("norm_out", norm_out_h, norm_out)
 
     barrier = pltpu.get_barrier_semaphore()
     for d in range(1, NZ):
@@ -139,11 +137,9 @@
 
     ready("tokens", "norm_in")
     normed = norm(tokens[...].astype(F32), norm_in[...]).astype(BF)
-    ready("wq")
+    ready("wq", "wk", "wv")
     queries = dot(normed, wq[...]).astype(BF)
-    ready("wk")
     fk[...] = dot_nt(normed, wk[...]).astype(BF)
-    ready("wv")
     fv[...] = dot_nt(normed, wv[...]).astype(BF)
 
     half = pl.ds(pl.multiple_of(c * 128, 128), 128)
@@ -172,8 +168,8 @@
     picked = jnp.where(head_of, dot(expand, queries), 0.0).astype(BF)
     grid = jnp.where(seq_of, dot(picked, fold), 0.0).astype(BF)
     parts = []
+    ready(*(("k", b) for b in range(4)))
     for b in range(4):
-        ready(("k", b))
         parts.append(dot(grid[16 * b : 16 * b + 16], kb[b]))
     scores = jnp.concatenate(parts, axis=0) * 0.125
     ready("lens", "bias")
@@ -203,8 +199,12 @@
         carry = carry + w[:, 0:1]
     stick = jnp.concatenate(sticks, axis=1)
     parts = []
+    ready(*(("v", b) for b in range(4)))
+    fetch("eg", eg_h, eg)
+    fetch("eu", eu_h, eu)
+    fetch("ed", ed_h, ed)
+    fetch("norm_out", norm_out_h, norm_out)
     for b in range(4):
-        ready(("v", b))
         parts.append(dot_nt(stick[16 * b : 16 * b + 16], vb[b]))
     att = jnp.where(seq_of, jnp.concatenate(parts, axis=0), 0.0).astype(BF)
     att = jnp.where(head_of, dot(att, fold), 0.0).astype(BF)
@@ -220,26 +220,23 @@
     ahead = ones_where(
         (rows((64, 64)) < cols((64, 64))) & (rows((64, 64)) // 16 == cols((64, 64)) // 16)
     )
-    for w in range(2):
-        table = jnp.zeros((16, 64), F32)
-        for j in range(4):
-            table = jnp.where(cols((16, 64)) // 16 == j, rtb[4 * w + j][:, 0:64], table)
-        hit = jnp.zeros(shape, F32)
-        share = jnp.zeros(shape, F32)
-        for k in range(6):
-            same = table[k : k + 1] == expert
-            hit = jnp.where(same, 1.0, hit)
-            share = jnp.where(same, table[8 + k : 9 + k], share)
-        rank = dot(hit.astype(BF), ahead)
-        here = (
-            (hit > 0.5)
-            & (rank == lax.rem(rows(shape), 2).astype(F32))
-            & (cols(shape) // 16 == lax.rem(rows(shape), 8) // 2)
-        )
-        pm[w] = ones_where(here)
-        high, low = halves(jnp.transpose(jnp.where(here, share, 0.0)))
-        wh[w] = high
-        wl[w] = low
+    table = jnp.zeros((16, 64), F32)
+    for j in range(4):
+        table = jnp.where(cols((16, 64)) // 16 == j, rtb[4 * c + j][:, 0:64], table)
+    hit = jnp.zeros(shape, F32)
+    share = jnp.zeros(shape, F32)
+    for k in range(6):
+        same = table[k : k + 1] == expert
+        hit = jnp.where(same, 1.0, hit)
+        share = jnp.where(same, table[8 + k : 9 + k], share)
+    rank = dot(hit.astype(BF), ahead)
+    here = (
+        (hit > 0.5)
+        & (rank == lax.rem(rows(shape), 2).astype(F32))
+        & (cols(shape) // 16 == lax.rem(rows(shape), 8) // 2)
+    )
+    pm[...] = ones_where(here)
+    wh[...], wl[...] = halves(jnp.transpose(jnp.where(here, share, 0.0)))
     await_bytes(rtb.at[1:8], flag("ts"))
     await_bytes(dwb.at[0:15], flag("ws"))
 
@@ -249,149 +246,169 @@
     await_bytes(ppr, flag("pr"))
     hidden = norm(normed.astype(F32) + (pps[...] + ppr[...]), norm_mid[...]).astype(BF)
     hb[...] = hidden
-    for d in (4, 1, 7, 3, 5, 2, 6):
-        t = SLOT[NZ - d]
-        send(hb.at[:, own_half], zb.at[t], flag("zs"), flag("zr", t // 4), along(d))
-    zb[0] = hb[:, own_half]
+    for f in range(NC):
+        source = hb.at[:, pl.ds(pl.multiple_of(c * 1024 + f * HW, HW), HW)]
+        lanes = pl.ds(pl.multiple_of(c * HW, HW), HW)
+        for d in (4, 1, 7, 3, 5, 2, 6):
+            t = SLOT[NZ - d]
+            there = (lax.rem(z + d, NZ), y, x, t // 4)
+            send(source, zb.at[f, t % 4, :, lanes], flag("zs"), flag("zr", f), there)
+
+    @pl.when(c == 0)
+    def _():
+        for f in range(NC):
+            for h in range(2):
+                at = 1024 * h + HW * f
+                zb[f, 0, :, HW * h : HW * h + HW] = hb[:, at : at + HW]
+
     mixing = jax.nn.sigmoid(jnp.sum(hidden.astype(F32) * mix_gate[...], -1, keepdims=True))
     await_bytes(pps, flag("ps"))
-
-    def dispatch(w):
-        await_bytes(zb.at[1:4] if w == 0 else zb.at[4:8], flag("zr", w))
-        block = zb[4 * w : 4 * w + 4].reshape(64, 1024)
-        going = dot(pm[w], block)
+    ready("eg", "eu", "ed")
+    send(eg, egm, flag("g0s"), flag("g0r"), mate)
+    send(eu, eum, flag("g1s"), flag("g1r"), mate)
+    send(ed, edm, flag("g2s"), flag("g2r"), mate)
+
+    for f in range(NC):
+
+        @pl.when(c == 0)
+        def _():
+            await_bytes(zb.at[f, 1:4], flag("zr", f))
+
+        @pl.when(c == 1)
+        def _():
+            await_bytes(zb.at[f], flag("zr", f))
+
+        going = dot(pm[...], zb[f].reshape(64, 2 * HW))
         for q in range(PLANE):
-            ob[w, q] = going[8 * q : 8 * q + 8].astype(BF)
+            ob[f, q] = going[8 * q : 8 * q + 8].astype(BF)
         for k in range(NP):
-            send(
-                ob.at[w, place(k)], xb.at[w, me], flag("xs", w), flag("xr", w, BACK[k]), across(k)
-            )
-        send(ob.at[w, me], yb.at[w, me], flag("ys", w), flag("yr", w), mate)
-        xb[w, me] = ob[w, me]
-
-    def forward(w):
-        for k in range(NP):
-            slot = place(k)
-            await_bytes(xb.at[w, slot], flag("xr", w, k))
-            send(xb.at[w, slot], yb.at[w, slot], flag("ys", w), flag("yr", w), mate)
-
-    def experts(w):
-        if w == 0:
-            ready("eg", "eu", "ed")
-        mine = xb[w].reshape(128, 1024)
-        gate = dot(mine, eg[own_half, :])
-        up = dot(mine, eu[own_half, :])
-        await_bytes(xb.at[w, 0:15], flag("xs", w))
-        await_bytes(yb.at[w], flag("yr", w))
-        other = yb[w].reshape(128, 1024)
-        gate = gate + dot(other, eg[mate_half, :])
-        up = up + dot(other, eu[mate_half, :])
-        act = (jax.nn.silu(gate) * up).astype(BF)
-        pbs[w] = dot(act, ed[:, mate_half]).astype(BF)
-        send(pbs.at[w], pbr.at[w], flag("bs", w), flag("br", w), mate)
-        part = dot(act, ed[:, own_half]).astype(BF)
-        await_bytes(yb.at[w], flag("ys", w))
-        return part
-
-    def give_back(w, part):
-        await_bytes(pbr.at[w], flag("br", w))
-        total = part.astype(F32) + pbr[w].astype(F32)
-        for q in range(PLANE):
-            eb[w, q] = total[8 * q : 8 * q + 8].astype(BF)
-        for k in range(NP):
-            send(eb.at[w, place(k)], rb.at[w, me], flag("es", w), flag("er", w), across(k))
-        rb[w, me] = eb[w, me]
-        await_bytes(pbr.at[w], flag("bs", w))
-
-    def combine(w):
-        await_bytes(rb.at[w, 0:15], flag("er", w))
-        block = rb[w].reshape(128, 1024)
-        part = dot(wh[w], block) + dot(wl[w], block)
-        for j in range(4):
-            s = 4 * w + j
-            piece = part[16 * j : 16 * j + 16]
-            if s == 0:
-                acc[...] = piece
-            else:
-                d = ORDER[s]
-                fs[s] = piece.astype(BF)
-                send(fs.at[s], fb.at[SLOT[NZ - d]], flag("fs", w), flag("fr", w), along(d))
-        await_bytes(rb.at[w, 0:15], flag("es", w))
-
-    dispatch(0)
-    dispatch(1)
-
-    holder = c == z // 4
-    features = pl.ds(pl.multiple_of(lax.rem(z, 4) * 256, 256), 256)
-
-    @pl.when(holder)
-    def _():
-        send(zb.at[:, :, features], tb, flag("cs"), flag("cr"), mate)
-        tb[...] = zb[:, :, features]
-        await_bytes(tb, flag("cs"))
-
+            send(ob.at[f, place(k)], xb.at[f, me], flag("xs", f), flag("xr", f), across(k))
+        xb[f, me] = ob[f, me]
+
+    inner = lax.rem(z, 4) * 256
+    chunk = inner // HW
+    features = pl.ds(pl.multiple_of((z // 4) * HW + lax.rem(inner, HW), 256), 256)
+    own_group = pl.ds(4 * c, 4)
+    mate_group = pl.ds(4 * o, 4)
+    send(zb.at[chunk, :, :, features], tb.at[own_group], flag("cs"), flag("cr"), mate)
+    tb[own_group] = zb[chunk, :, :, features]
     await_bytes(dwb.at[0:15], flag("wr"))
-
-    @pl.when(jnp.logical_not(holder))
-    def _():
-        await_bytes(tb, flag("cr"))
-
+    await_bytes(tb.at[mate_group], flag("cr"))
     column = tb[...].reshape(128, 256)
     pre = dot(column, dwb[:, 0:16, :].reshape(256, 128))
     lin = dot(column, dwb[:, 16:32, :].reshape(256, 128))
     for s in range(NZ):
-        d2s[s, :, 0:128] = pre[16 * s : 16 * s + 16]
-        d2s[s, :, 128:256] = lin[16 * s : 16 * s + 16]
+        d2s[s, :, 0:128] = pre[16 * s : 16 * s + 16].astype(BF)
+        d2s[s, :, 128:256] = lin[16 * s : 16 * s + 16].astype(BF)
     for d in ORDER[1:]:
         send(d2s.at[SLOT[d]], d2b.at[SLOT[NZ - d]], flag("d2s"), flag("d2r"), along(d))
     d2b[0] = d2s[0]
-
-    forward(0)
-    part0 = experts(0)
-    give_back(0, part0)
-    await_bytes(zb.at[1:8], flag("zs"))
-    forward(1)
-    part1 = experts(1)
+    await_bytes(tb.at[own_group], flag("cs"))
+    await_bytes(fb.at[:, 1:8], flag("zs"))
+    await_bytes(egm, flag("g0s"))
+    await_bytes(eum, flag("g1s"))
+    await_bytes(edm, flag("g2s"))
+    await_bytes(egm, flag("g0r"))
+    await_bytes(eum, flag("g1r"))
+    await_bytes(edm, flag("g2r"))
+
+    sums = [None] * 4
+    for f in range(NC):
+        await_bytes(xb.at[f, 0:15], flag("xr", f))
+        arrived = xb[f].reshape(128, 2 * HW)
+        for i, ref in enumerate((eg, eu, egm, eum)):
+            step = dot(arrived[:, 0:HW], ref[HW * f : HW * f + HW])
+            step = step + dot(arrived[:, HW : 2 * HW], ref[1024 + HW * f : 1024 + HW * f + HW])
+            if f > 0:
+                step = step + ga[i]
+            if f < NC - 1:
+                ga[i] = step
+            sums[i] = step
+    acts = [(jax.nn.silu(sums[i]) * sums[i + 1]).astype(BF) for i in (0, 2)]
+    for f in range(NC):
+        for h in range(2):
+            at = 1024 * h + HW * f
+            total = dot(acts[0], ed[:, at : at + HW]).astype(BF).astype(F32)
+            total = total + dot(acts[1], edm[:, at : at + HW]).astype(BF).astype(F32)
+            for q in range(PLANE):
+                eb[f, q, :, HW * h : HW * h + HW] = total[8 * q : 8 * q + 8].astype(BF)
+        for k in range(NP):
+            send(eb.at[f, place(k)], rb.at[f, me], flag("es", f), flag("er", f), across(k))
+        rb[f, me] = eb[f, me]
+    for f in range(NC):
+        await_bytes(xb.at[f, 0:15], flag("xs", f))
 
     await_bytes(d2b.at[1:8], flag("d2r"))
-    total = jnp.sum(d2b[...], axis=0)
-    das[...] = (jax.nn.silu(total[:, 0:128]) * total[:, 128:256]).astype(BF)
+    summed = jnp.sum(d2b[...].astype(F32), axis=0)
+    das[...] = (jax.nn.silu(summed[:, 0:128]) * summed[:, 128:256]).astype(BF)
     for d in ORDER[1:]:
         send(das, dab.at[SLOT[NZ - d]], flag("d3s"), flag("d3r"), along(d))
     dab[0] = das[...]
-
-    give_back(1, part1)
-    combine(0)
-
     await_bytes(d2b.at[1:8], flag("d2s"))
-    await_bytes(dab.at[1:8], flag("d3r"))
-    cols_out = dot_nt(dab[...].reshape(128, 128), dwb[:, 32:48, :].reshape(256, 128))
-    for s in range(NZ):
-        d4s[s] = cols_out[16 * s : 16 * s + 16]
-    for d in ORDER[1:]:
-        send(d4s.at[SLOT[d]], d4b.at[z], flag("d4s"), flag("d4r"), along(d))
-    d4b[z] = d4s[0]
-    await_bytes(dab.at[1:8], flag("d3s"))
-
-    combine(1)
+
+    def combine(f, group):
+        await_bytes(rb.at[f, 0:15], flag("er", f))
+        block = rb[f].reshape(128, 2 * HW)
+        part = dot(wh[...], block) + dot(wl[...], block)
+        for j in range(4):
+            d = ORDER[4 * group + j]
+            fs[f, j] = part[16 * j : 16 * j + 16].astype(BF)
+            if d == 0:
+                send(fs.at[f, j, :, HW : 2 * HW], fb.at[f, 0], flag("fs"), flag("fr", f), mate)
+                fb[f, 0] = fs[f, j, :, 0:HW]
+                continue
+            for h in range(2):
+                there = (lax.rem(z + d, NZ), y, x, h)
+                piece = fs.at[f, j, :, HW * h : HW * h + HW]
+                send(piece, fb.at[f, SLOT[NZ - d]], flag("fs"), flag("fr", f), there)
+        await_bytes(rb.at[f, 0:15], flag("es", f))
+
+    for f in range(NC):
+        pl.when(c == 0)(lambda: combine(f, 0))
+        pl.when(c == 1)(lambda: combine(f, 1))
+        if f == 0:
+            await_bytes(dab.at[1:8], flag("d3r"))
+            block = dot_nt(dab[...].reshape(128, 128), dwb[:, 32:48, :].reshape(256, 128))
+            for s in range(NZ):
+                d4s[s] = block[16 * s : 16 * s + 16].astype(BF)
+            for d in ORDER[1:]:
+                send(d4s.at[SLOT[d]], d4b.at[z], flag("d4s"), flag("d4r"), along(d))
+            d4b[z] = d4s[0]
+            await_bytes(dab.at[1:8], flag("d3s"))
+
     await_bytes(d4b.at[0:7], flag("d4r"))
     send(d4b, d4p, flag("d5s"), flag("d5r"), mate)
     ready("norm_out")
-    await_bytes(fb.at[1:4], flag("fr", 0))
-    total = acc[...] + fb[1].astype(F32) + fb[2].astype(F32) + fb[3].astype(F32)
-    await_bytes(d4p, flag("d5r"))
-    mixed = hidden.astype(F32) + mixing * jnp.concatenate(
-        [d4b[n] + d4p[n] for n in range(NZ)], axis=1
-    )
     await_bytes(d4b.at[0:7], flag("d4s"))
-    await_bytes(d4p, flag("d5s"))
-    await_bytes(fb.at[1:4], flag("fs", 0))
-    await_bytes(fb.at[4:8], flag("fr", 1))
-    for s in range(4, NZ):
-        total = total + fb[s].astype(F32)
-    fin[:, own_half] = total
-    send(fin.at[:, own_half], fin.at[:, own_half], flag("us"), flag("ur"), mate)
-    await_bytes(fb.at[4:8], flag("fs", 1))
+
+    for f in range(NC):
+
+        @pl.when(c == 0)
+        def _():
+            await_bytes(fb.at[f, 1:8], flag("fr", f))
+
+        @pl.when(c == 1)
+        def _():
+            await_bytes(fb.at[f], flag("fr", f))
+
+        piece = pl.ds(pl.multiple_of(c * 1024 + HW * f, HW), HW)
+        fin[:, piece] = jnp.sum(fb[f].astype(F32), axis=0)
+        send(fin.at[:, piece], fin.at[:, piece], flag("us"), flag("ur"), mate)
+        if f == 0:
+            await_bytes(d4p, flag("d5r"))
+            mixed = hidden.astype(F32) + mixing * jnp.concatenate(
+                [d4b[n].astype(F32) + d4p[n].astype(F32) for n in range(NZ)], axis=1
+            )
+            await_bytes(d4p, flag("d5s"))
+
+    @pl.when(c == 0)
+    def _():
+        await_bytes(fb.at[:, 0:7], flag("fs"))
+
+    @pl.when(c == 1)
+    def _():
+        await_bytes(fb, flag("fs"))
+
     await_bytes(fin.at[:, mate_half], flag("ur"))
     out[...] = norm(mixed + fin[...], norm_out[...]).astype(BF)
     await_bytes(fin.at[:, own_half], flag("us"))
@@ -433,36 +450,36 @@
             V((2048, 256), BF),
             V((256, 2048), BF),
             V((1, 2048), F32),
+            V((2048, 256), BF),
+            V((2048, 256), BF),
+            V((256, 2048), BF),
             V((16, 2048), BF),
             V((16, 2048), F32),
             V((16, 2048), F32),
-            V((8, 16, 1024), BF),
-            V((2, 16, 8, 1024), BF),
-            V((2, 16, 8, 1024), BF),
-            V((2, 16, 8, 1024), BF),
-            V((2, 128, 1024), BF),
-            V((2, 128, 1024), BF),
-            V((2, 16, 8, 1024), BF),
-            V((2, 16, 8, 1024), BF),
-            V((8, 16, 1024), BF),
-            V((8, 16, 1024), BF),
-            V((16, 1024), F32),
+            V((NC, 4, 16, 2 * HW), BF),
+            V((NC, 16, 8, 2 * HW), BF),
+            V((NC, 16, 8, 2 * HW), BF),
+            V((NC, 16, 8, 2 * HW), BF),
+            V((NC, 16, 8, 2 * HW), BF),
+            V((NC, 4, 16, 2 * HW), BF),
+            V((NC, 8, 16, HW), BF),
             V((16, 2048), F32),
             V((16, 128), F32),
             V((8, 16, 128), F32),
             V((48, 128), BF),
             V((16, 48, 128), BF),
             V((8, 16, 256), BF),
-            V((8, 16, 256), F32),
-            V((8, 16, 256), F32),
+            V((8, 16, 256), BF),
+            V((8, 16, 256), BF),
             V((16, 128), BF),
             V((8, 16, 128), BF),
-            V((8, 16, 256), F32),
-            V((8, 16, 256), F32),
-            V((8, 16, 256), F32),
-            V((2, 128, 64), BF),
-            V((2, 64, 128), BF),
-            V((2, 64, 128), BF),
+            V((8, 16, 256), BF),
+            V((8, 16, 256), BF),
+            V((8, 16, 256), BF),
+            V((128, 64), BF),
+            V((64, 128), BF),
+            V((64, 128), BF),
+            V((4, 128, 256), F32),
             dma((27,)),
             dma((96,)),
         ],

time: 54.1 us -> 51.3 us (0.948)
  Pallas kernels: 51.6 us -> 48.7 us
    pallas_call x1, Pallas kernels: 51.6 us -> 48.7 us  [shards(): pl.pallas_call(body, out_shape=(V((16, 2048), BF), V((16, 64), BF), V((16...]
where the time goes in v3:
time: 51.3 us; the launch traced here: 51.2 us
  Pallas kernels  48.7 us (95%)
  local copies, waits for them, and re-layouts  1.82 us (4%)
  between operations  0.65 us (1%)
    pallas_call x1, Pallas kernels, shards(): pl.pallas_call(body, out_shape=(V((16, 2048), BF), V((16, 64), BF), V((16...  48.7 us
    unnamed x3, local copies, waits for them, and re-layouts  1.82 us

profile of v3, /device:TPU:1, one launch (start us, length us, event | category | flops | bytes accessed | tf_op | source)
XLA Modules:
  0.0 51.2 jit_solution(6486993095179911115)
XLA Ops:
  0.6 48.7 %shard_map.220 = (bf16[16,2048]{1,0:T(8,128)(2,1)S(1)}, bf16[16,64]{1,0:T(8,128)(2,1)S(1)}, bf16[16,64]{1,0:T(8,128)(2,1)S(1)}) custom-call(bf16[16,2048]{1,0:T(8,128)(2,1)} %tokens_h.1, f32[1,2048]{1,0:T(1,128)} %bitcast.21, bf16[2048,256]{1,0:T(8,128)(2,1)} %wq_h.1, bf16[64,2048]{1,0:T(8,128)(2,1)} %bitcast.19, bf16[64,2048]{1,0:T(8,128)(2,1)} %bitcast.20, ...), custom_call_target="tpu_custom_call" | custom-call | tf_op jit(solution)/shard_map/pallas_call | solution.py:426
  49.4 0.6 %copy.27 = bf16[16,2048]{1,0:T(8,128)(2,1)} copy(bf16[16,2048]{1,0:T(8,128)(2,1)S(1)} %get-tuple-element.3) | data formatting | bytes 131072
  50.0 0.6 %copy.28 = bf16[16,64]{1,0:T(8,128)(2,1)} copy(bf16[16,64]{1,0:T(8,128)(2,1)S(1)} %get-tuple-element.4) | data formatting | bytes 4096
  50.6 0.6 %copy.29 = bf16[16,64]{1,0:T(8,128)(2,1)} copy(bf16[16,64]{1,0:T(8,128)(2,1)S(1)} %get-tuple-element.5) | data formatting | bytes 4096

commit v4 on v3

--- a/solution.py
+++ b/solution.py
@@ -12,11 +12,11 @@
 F32 = jnp.float32
 NZ, NY, NX = 8, 4, 4
 PLANE = NY * NX
-ORDER = (0, 4, 1, 7, 2, 6, 3, 5)
+ORDER = (0, 1, 7, 2, 6, 3, 5, 4)
 SLOT = {d: i for i, d in enumerate(ORDER)}
 OFFS = sorted(
     ((dy, dx) for dy in range(NY) for dx in range(NX) if (dy, dx) != (0, 0)),
-    key=lambda o: min(o[0], NY - o[0]) + min(o[1], NX - o[1]),
+    key=lambda o: -min(o[0], NY - o[0]) - min(o[1], NX - o[1]),
 )
 BACK = [OFFS.index(((-dy) % NY, (-dx) % NX)) for dy, dx in OFFS]
 NP = len(OFFS)
@@ -59,14 +59,15 @@
 def body(
     tokens_h, norm_in_h, wq_h, wk_h, wv_h, lens_h, bias_h, ck, cv, dgate_h, dup_h, ddown_h,
     routes_h, weights_h, wo_h, norm_mid_h, mix_gate_h, eg_h, eu_h, ed_h, norm_out_h,
-    out, fk, fv,
+    res,
     tokens, norm_in, wq, wk, wv, lens, bias, kb, vb, dgate, dup, ddown,
     routes, weights, wo, norm_mid, mix_gate, eg, eu, ed, norm_out,
     egm, eum, edm, hb, pps, ppr, zb, ob, xb, eb, rb, fs, fb, fin,
-    rts, rtb, dws, dwb, tb, d2s, d2b, das, dab, d4s, d4b, d4p,
+    rts, rtb, dws, dwb, d2s, d2b, das, dab, d3m, d4s, d4b,
     pm, wh, wl, ga,
     lsem, bank,
 ):
+    out, fk, fv = res.at[:, 0:2048], res.at[:, 2048:2112], res.at[:, 2176:2240]
     z, y, x, c = (lax.axis_index(a) for a in (*EP, "tp"))
     me = y * NX + x
     o = 1 - c
@@ -142,11 +143,10 @@
     fk[...] = dot_nt(normed, wk[...]).astype(BF)
     fv[...] = dot_nt(normed, wv[...]).astype(BF)
 
-    half = pl.ds(pl.multiple_of(c * 128, 128), 128)
     ready("dgate", "dup", "ddown", "routes", "weights")
-    dws[0:16] = dgate[:, half]
-    dws[16:32] = dup[:, half]
-    dws[32:48] = ddown[:, half]
+    dws[0:16] = dgate[...]
+    dws[16:32] = dup[...]
+    dws[32:48] = ddown[...]
     rts[...] = jnp.zeros((16, 128), F32)
     for j in range(8):
         rts[0:6, 16 * j : 16 * j + 16] = routes[...].astype(F32)
@@ -246,13 +246,12 @@
     await_bytes(ppr, flag("pr"))
     hidden = norm(normed.astype(F32) + (pps[...] + ppr[...]), norm_mid[...]).astype(BF)
     hb[...] = hidden
-    for f in range(NC):
+    lanes = pl.ds(pl.multiple_of(c * HW, HW), HW)
+    for f, d in [(f, d) for f in range(NC) for d in (4, 3, 5, 2, 6, 1, 7)]:
         source = hb.at[:, pl.ds(pl.multiple_of(c * 1024 + f * HW, HW), HW)]
-        lanes = pl.ds(pl.multiple_of(c * HW, HW), HW)
-        for d in (4, 1, 7, 3, 5, 2, 6):
-            t = SLOT[NZ - d]
-            there = (lax.rem(z + d, NZ), y, x, t // 4)
-            send(source, zb.at[f, t % 4, :, lanes], flag("zs"), flag("zr", f), there)
+        t = SLOT[NZ - d]
+        there = (lax.rem(z + d, NZ), y, x, t // 4)
+        send(source, zb.at[f, t % 4, :, lanes], flag("zs"), flag("zr", f), there)
 
     @pl.when(c == 0)
     def _():
@@ -286,24 +285,34 @@
         xb[f, me] = ob[f, me]
 
     inner = lax.rem(z, 4) * 256
-    chunk = inner // HW
     features = pl.ds(pl.multiple_of((z // 4) * HW + lax.rem(inner, HW), 256), 256)
-    own_group = pl.ds(4 * c, 4)
-    mate_group = pl.ds(4 * o, 4)
-    send(zb.at[chunk, :, :, features], tb.at[own_group], flag("cs"), flag("cr"), mate)
-    tb[own_group] = zb[chunk, :, :, features]
+    column = zb[inner // HW, :, :, features].reshape(64, 256)
     await_bytes(dwb.at[0:15], flag("wr"))
-    await_bytes(tb.at[mate_group], flag("cr"))
-    column = tb[...].reshape(128, 256)
-    pre = dot(column, dwb[:, 0:16, :].reshape(256, 128))
-    lin = dot(column, dwb[:, 16:32, :].reshape(256, 128))
-    for s in range(NZ):
-        d2s[s, :, 0:128] = pre[16 * s : 16 * s + 16].astype(BF)
-        d2s[s, :, 128:256] = lin[16 * s : 16 * s + 16].astype(BF)
-    for d in ORDER[1:]:
-        send(d2s.at[SLOT[d]], d2b.at[SLOT[NZ - d]], flag("d2s"), flag("d2r"), along(d))
-    d2b[0] = d2s[0]
-    await_bytes(tb.at[own_group], flag("cs"))
+    pre = dot(column, dwb[:, 0:16, :].reshape(256, 256))
+    lin = dot(column, dwb[:, 16:32, :].reshape(256, 256))
+    for j in range(4):
+        for h in range(2):
+            for i, v in enumerate((pre, lin)):
+                at = 256 * h + 128 * i
+                d2s[j, :, at : at + 128] = v[16 * j : 16 * j + 16, 128 * h : 128 * h + 128].astype(BF)
+
+    def to_owners(group, source, target, name, width, f):
+        for j in range(4):
+            d = ORDER[4 * group + j]
+            for h in range(2):
+                piece = source.at[j, :, width * h : width * h + width]
+                slot = target.at[SLOT[(NZ - d) % NZ]]
+                if d:
+                    there = (lax.rem(z + d, NZ), y, x, h)
+                elif h:
+                    there = mate
+                else:
+                    target[0] = source[j, :, 0:width]
+                    continue
+                send(piece, slot, flag(name, "s"), flag(name, "r", f), there)
+
+    pl.when(c == 0)(lambda: to_owners(0, d2s, d2b, "d2", 256, 0))
+    pl.when(c == 1)(lambda: to_owners(1, d2s, d2b, "d2", 256, 0))
     await_bytes(fb.at[:, 1:8], flag("zs"))
     await_bytes(egm, flag("g0s"))
     await_bytes(eum, flag("g1s"))
@@ -338,79 +347,114 @@
     for f in range(NC):
         await_bytes(xb.at[f, 0:15], flag("xs", f))
 
-    await_bytes(d2b.at[1:8], flag("d2r"))
+    @pl.when(c == 0)
+    def _():
+        await_bytes(d2b.at[1:8], flag("d2", "r", 0))
+        await_bytes(d2b.at[1:8], flag("d2", "s"))
+
+    @pl.when(c == 1)
+    def _():
+        await_bytes(d2b, flag("d2", "r", 0))
+        await_bytes(d2b, flag("d2", "s"))
+
     summed = jnp.sum(d2b[...].astype(F32), axis=0)
     das[...] = (jax.nn.silu(summed[:, 0:128]) * summed[:, 128:256]).astype(BF)
+    lanes = pl.ds(pl.multiple_of(c * 128, 128), 128)
     for d in ORDER[1:]:
-        send(das, dab.at[SLOT[NZ - d]], flag("d3s"), flag("d3r"), along(d))
-    dab[0] = das[...]
-    await_bytes(d2b.at[1:8], flag("d2s"))
+        t = SLOT[NZ - d]
+        there = (lax.rem(z + d, NZ), y, x, t // 4)
+        send(das, dab.at[t % 4, :, lanes], flag("d3s"), flag("d3r"), there)
+
+    @pl.when(c == 0)
+    def _():
+        dab[0, :, 0:128] = das[...]
+
+    @pl.when(c == 1)
+    def _():
+        send(das, dab.at[0, :, 128:256], flag("d3s"), flag("d3r"), mate)
+
+    def dense_columns(group):
+        if group == 0:
+            await_bytes(d3m.at[0:7], flag("d3r"))
+            await_bytes(d3m.at[0:7], flag("d3s"))
+        else:
+            await_bytes(d3m, flag("d3r"))
+            await_bytes(d3m, flag("d3s"))
+        block = dot_nt(dab[...].reshape(64, 256), dwb[:, 32:48, :].reshape(256, 256))
+        spot = lax.rem(z, 4)
+        for j in range(4):
+            d = ORDER[4 * group + j]
+            d4s[j] = block[16 * j : 16 * j + 16].astype(BF)
+            if d:
+                there = (lax.rem(z + d, NZ), y, x, z // 4)
+                send(d4s.at[j], d4b.at[spot], flag("d4s"), flag("d4r"), there)
+                continue
+
+            @pl.when(z < 4)
+            def _():
+                d4b[spot] = d4s[j]
+
+            @pl.when(z >= 4)
+            def _():
+                send(d4s.at[j], d4b.at[spot], flag("d4s"), flag("d4r"), mate)
 
     def combine(f, group):
         await_bytes(rb.at[f, 0:15], flag("er", f))
         block = rb[f].reshape(128, 2 * HW)
         part = dot(wh[...], block) + dot(wl[...], block)
         for j in range(4):
-            d = ORDER[4 * group + j]
             fs[f, j] = part[16 * j : 16 * j + 16].astype(BF)
-            if d == 0:
-                send(fs.at[f, j, :, HW : 2 * HW], fb.at[f, 0], flag("fs"), flag("fr", f), mate)
-                fb[f, 0] = fs[f, j, :, 0:HW]
-                continue
-            for h in range(2):
-                there = (lax.rem(z + d, NZ), y, x, h)
-                piece = fs.at[f, j, :, HW * h : HW * h + HW]
-                send(piece, fb.at[f, SLOT[NZ - d]], flag("fs"), flag("fr", f), there)
+        to_owners(group, fs.at[f], fb.at[f], "f", HW, f)
         await_bytes(rb.at[f, 0:15], flag("es", f))
 
-    for f in range(NC):
-        pl.when(c == 0)(lambda: combine(f, 0))
-        pl.when(c == 1)(lambda: combine(f, 1))
-        if f == 0:
-            await_bytes(dab.at[1:8], flag("d3r"))
-            block = dot_nt(dab[...].reshape(128, 128), dwb[:, 32:48, :].reshape(256, 128))
-            for s in range(NZ):
-                d4s[s] = block[16 * s : 16 * s + 16].astype(BF)
-            for d in ORDER[1:]:
-                send(d4s.at[SLOT[d]], d4b.at[z], flag("d4s"), flag("d4r"), along(d))
-            d4b[z] = d4s[0]
-            await_bytes(dab.at[1:8], flag("d3s"))
-
-    await_bytes(d4b.at[0:7], flag("d4r"))
-    send(d4b, d4p, flag("d5s"), flag("d5r"), mate)
+    for group in range(2):
+
+        @pl.when(c == group)
+        def _():
+            for f in range(NC):
+                combine(f, group)
+            dense_columns(group)
+
     ready("norm_out")
-    await_bytes(d4b.at[0:7], flag("d4s"))
+    few = jnp.logical_and(c == 0, z < 4)
+
+    @pl.when(few)
+    def _():
+        await_bytes(d4b.at[0:3], flag("d4r"))
+        await_bytes(d4b.at[0:3], flag("d4s"))
+
+    @pl.when(jnp.logical_not(few))
+    def _():
+        await_bytes(d4b, flag("d4r"))
+        await_bytes(d4b, flag("d4s"))
+
+    dense = jnp.concatenate([d4b[n] for n in range(4)], axis=1).astype(F32)
+    dense = hb[:, own_half].astype(F32) + mixing * dense
 
     for f in range(NC):
 
         @pl.when(c == 0)
         def _():
-            await_bytes(fb.at[f, 1:8], flag("fr", f))
+            await_bytes(fb.at[f, 1:8], flag("f", "r", f))
 
         @pl.when(c == 1)
         def _():
-            await_bytes(fb.at[f], flag("fr", f))
+            await_bytes(fb.at[f], flag("f", "r", f))
 
         piece = pl.ds(pl.multiple_of(c * 1024 + HW * f, HW), HW)
-        fin[:, piece] = jnp.sum(fb[f].astype(F32), axis=0)
+        fin[:, piece] = jnp.sum(fb[f].astype(F32), axis=0) + dense[:, HW * f : HW * f + HW]
         send(fin.at[:, piece], fin.at[:, piece], flag("us"), flag("ur"), mate)
-        if f == 0:
-            await_bytes(d4p, flag("d5r"))
-            mixed = hidden.astype(F32) + mixing * jnp.concatenate(
-                [d4b[n].astype(F32) + d4p[n].astype(F32) for n in range(NZ)], axis=1
-            )
-            await_bytes(d4p, flag("d5s"))
 
     @pl.when(c == 0)
     def _():
-        await_bytes(fb.at[:, 0:7], flag("fs"))
+        await_bytes(fb.at[:, 0:7], flag("f", "s"))
 
     @pl.when(c == 1)
     def _():
-        await_bytes(fb, flag("fs"))
+        await_bytes(fb, flag("f", "s"))
 
     await_bytes(fin.at[:, mate_half], flag("ur"))
-    out[...] = norm(mixed + fin[...], norm_out[...]).astype(BF)
+    out[...] = norm(fin[...], norm_out[...]).astype(BF)
     await_bytes(fin.at[:, own_half], flag("us"))
 
 
@@ -423,11 +467,11 @@
     hbm = pl.BlockSpec(memory_space=pltpu.HBM)
     dma = pltpu.SemaphoreType.DMA
     V = pltpu.VMEM
-    return pl.pallas_call(
+    res = pl.pallas_call(
         body,
-        out_shape=(V((16, 2048), BF), V((16, 64), BF), V((16, 64), BF)),
+        out_shape=V((16, 2304), BF),
         in_specs=[hbm] * 21,
-        out_specs=(vmem, vmem, vmem),
+        out_specs=vmem,
         scratch_shapes=[
             V((16, 2048), BF),
             V((1, 2048), F32),
@@ -466,16 +510,15 @@
             V((16, 2048), F32),
             V((16, 128), F32),
             V((8, 16, 128), F32),
-            V((48, 128), BF),
-            V((16, 48, 128), BF),
-            V((8, 16, 256), BF),
-            V((8, 16, 256), BF),
+            V((48, 256), BF),
+            V((16, 48, 256), BF),
+            V((4, 16, 512), BF),
             V((8, 16, 256), BF),
             V((16, 128), BF),
+            V((4, 16, 256), BF),
             V((8, 16, 128), BF),
-            V((8, 16, 256), BF),
-            V((8, 16, 256), BF),
-            V((8, 16, 256), BF),
+            V((4, 16, 256), BF),
+            V((4, 16, 256), BF),
             V((128, 64), BF),
             V((64, 128), BF),
             V((64, 128), BF),
@@ -509,6 +552,7 @@
         expert_down.reshape(256, 2048),
         norm_out.reshape(1, -1),
     )
+    return res[:, 0:2048], res[:, 2048:2112], res[:, 2176:2240]
 
 
 def solution(mesh):

time: 51.3 us -> 48.3 us (0.942)
  Pallas kernels: 48.7 us -> 46.4 us
  local copies, waits for them, and re-layouts: 1.82 us -> 1.23 us
    pallas_call x1, Pallas kernels: 48.7 us -> 46.4 us  [shards(): pl.pallas_call(body, out_shape=V((16, 2304), BF), in_specs=[hbm] * 21, ou...]
    unnamed x3 -> x0, local copies, waits for them, and re-layouts: 1.82 us -> none
    slice x0 -> x2, local copies, waits for them, and re-layouts: none -> 1.23 us  [shards(): return (res[:, 0:2048], res[:, 2048:2112], res[:, 2176:2240])]
where the time goes in v4:
time: 48.3 us; the launch traced here: 48.2 us
  Pallas kernels  46.4 us (96%)
  local copies, waits for them, and re-layouts  1.23 us (3%)
  between operations  0.65 us (1%)
    pallas_call x1, Pallas kernels, shards(): pl.pallas_call(body, out_shape=V((16, 2304), BF), in_specs=[hbm] * 21, ou...  46.4 us
    slice x2, local copies, waits for them, and re-layouts, shards(): return (res[:, 0:2048], res[:, 2048:2112], res[:, 2176:2240])  1.23 us

profile of v4, /device:TPU:1, one launch (start us, length us, event | category | flops | bytes accessed | tf_op | source)
XLA Modules:
  0.0 48.2 jit_solution(17320630158015055358)
XLA Ops:
  0.6 46.4 %shard_map.220 = bf16[16,2304]{1,0:T(8,128)(2,1)S(1)} custom-call(bf16[16,2048]{1,0:T(8,128)(2,1)} %tokens_h.1, f32[1,2048]{1,0:T(1,128)} %bitcast.21, bf16[2048,256]{1,0:T(8,128)(2,1)} %wq_h.1, bf16[64,2048]{1,0:T(8,128)(2,1)} %bitcast.19, bf16[64,2048]{1,0:T(8,128)(2,1)} %bitcast.20, s32[16]{0:T(128)} %lens_h.1, f32[4]{0:T(128)} %bias_h.1, ...), custom_call_target="tpu_custom_call" | custom-call | tf_op jit(solution)/shard_map/pallas_call | solution.py:470
  47.0 0.6 %fusion = (bf16[16,64]{1,0:T(8,128)(2,1)}, bf16[16,64]{1,0:T(8,128)(2,1)}) fusion(bf16[16,2304]{1,0:T(8,128)(2,1)S(1)} %shard_map.220), kind=kLoop, calls=%fused_computation | loop fusion | bytes 8192 | tf_op jit(solution)/shard_map/slice | solution.py:555
  47.6 0.6 %slice.9 = bf16[16,2048]{1,0:T(8,128)(2,1)} slice(bf16[16,2304]{1,0:T(8,128)(2,1)S(1)} %shard_map.220), slice={[0:16], [0:2048]} | slice | bytes 131072 | tf_op jit(solution)/shard_map/slice | solution.py:555

commit v5 on v4

--- a/solution.py
+++ b/solution.py
@@ -16,7 +16,7 @@
 SLOT = {d: i for i, d in enumerate(ORDER)}
 OFFS = sorted(
     ((dy, dx) for dy in range(NY) for dx in range(NX) if (dy, dx) != (0, 0)),
-    key=lambda o: -min(o[0], NY - o[0]) - min(o[1], NX - o[1]),
+    key=lambda o: (-min(o[0], NY - o[0]) - min(o[1], NX - o[1]), (o[0] + o[1]) % 2, o[1]),
 )
 BACK = [OFFS.index(((-dy) % NY, (-dx) % NX)) for dy, dx in OFFS]
 NP = len(OFFS)
@@ -247,7 +247,7 @@
     hidden = norm(normed.astype(F32) + (pps[...] + ppr[...]), norm_mid[...]).astype(BF)
     hb[...] = hidden
     lanes = pl.ds(pl.multiple_of(c * HW, HW), HW)
-    for f, d in [(f, d) for f in range(NC) for d in (4, 3, 5, 2, 6, 1, 7)]:
+    for f, d in [(f, d) for f in range(NC) for d in (4, 5, 3, 6, 2, 7, 1)]:
         source = hb.at[:, pl.ds(pl.multiple_of(c * 1024 + f * HW, HW), HW)]
         t = SLOT[NZ - d]
         there = (lax.rem(z + d, NZ), y, x, t // 4)
@@ -297,7 +297,7 @@
                 d2s[j, :, at : at + 128] = v[16 * j : 16 * j + 16, 128 * h : 128 * h + 128].astype(BF)
 
     def to_owners(group, source, target, name, width, f):
-        for j in range(4):
+        for j in (3, 2, 1, 0):
             d = ORDER[4 * group + j]
             for h in range(2):
                 piece = source.at[j, :, width * h : width * h + width]

time: 48.3 us -> 48.1 us (level)
  no operation moved by 1% of the time
where the time goes in v5:
time: 48.1 us; the launch traced here: 48 us
  Pallas kernels  46.1 us (96%)
  local copies, waits for them, and re-layouts  1.23 us (3%)
  between operations  0.65 us (1%)
    pallas_call x1, Pallas kernels, shards(): pl.pallas_call(body, out_shape=V((16, 2304), BF), in_specs=[hbm] * 21, ou...  46.1 us
    slice x2, local copies, waits for them, and re-layouts, shards(): return (res[:, 0:2048], res[:, 2048:2112], res[:, 2176:2240])  1.23 us

profile of v5, /device:TPU:1, one launch (start us, length us, event | category | flops | bytes accessed | tf_op | source)
XLA Modules:
  0.0 48.0 jit_solution(14748948298280610643)
XLA Ops:
  0.6 46.1 %shard_map.220 = bf16[16,2304]{1,0:T(8,128)(2,1)S(1)} custom-call(bf16[16,2048]{1,0:T(8,128)(2,1)} %tokens_h.1, f32[1,2048]{1,0:T(1,128)} %bitcast.21, bf16[2048,256]{1,0:T(8,128)(2,1)} %wq_h.1, bf16[64,2048]{1,0:T(8,128)(2,1)} %bitcast.19, bf16[64,2048]{1,0:T(8,128)(2,1)} %bitcast.20, s32[16]{0:T(128)} %lens_h.1, f32[4]{0:T(128)} %bias_h.1, ...), custom_call_target="tpu_custom_call" | custom-call | tf_op jit(solution)/shard_map/pallas_call | solution.py:470
  46.8 0.6 %fusion = (bf16[16,64]{1,0:T(8,128)(2,1)}, bf16[16,64]{1,0:T(8,128)(2,1)}) fusion(bf16[16,2304]{1,0:T(8,128)(2,1)S(1)} %shard_map.220), kind=kLoop, calls=%fused_computation | loop fusion | bytes 8192 | tf_op jit(solution)/shard_map/slice | solution.py:555
  47.4 0.6 %slice.9 = bf16[16,2048]{1,0:T(8,128)(2,1)} slice(bf16[16,2304]{1,0:T(8,128)(2,1)S(1)} %shard_map.220), slice={[0:16], [0:2048]} | slice | bytes 131072 | tf_op jit(solution)/shard_map/slice | solution.py:555
